TPU v7x, 32 devices: a whole 2x2x4 slice. The times are simulated.
32 devices in a mesh: ep: 8 (over z, core), tp: 4 (over y, x).
Axes of the slice: x: 2, y: 2, z: 4, core: 2. Of those that a mesh axis runs over, the one named last changes fastest.
Arguments:
- query_maps: bfloat16 [2048, 4096], P('ep', 'tp'), may hold values from -40 to 40
- key_maps: bfloat16 [2048, 4096], P('ep', 'tp'), may hold values from -40 to 40
- value_rows: bfloat16 [2048, 4096], P('ep', 'tp'), may hold values from -6 to 6
- head_lambda: float32 [16], P('tp'), may hold values from 0.3 to 0.8
- head_gain: float32 [256], replicated, may hold values from 0.1 to 1.9
- out_weight: bfloat16 [4096, 2048], P('tp'), may hold values from -0.125 to 0.125
- expert_rows: bfloat16 [1024, 2048], P('ep'), may hold values from -6 to 6
- expert_gain: float32 [2048], replicated, may hold values from 0.1 to 1.9
- routes: int32 [1024, 2], P('ep'), may hold values from 0 to 7, all different within a row; in each aligned block of 128 rows (0 to 127, 128 to 255, ...) at most 48 rows name the same one
- route_weights: float32 [1024, 2], P('ep'), may hold values from 0.2 to 1
- gate_weight: bfloat16 [8, 2048, 4096], P('ep', None, 'tp'), may hold values from -0.125 to 0.125
- up_weight: bfloat16 [8, 2048, 4096], P('ep', None, 'tp'), may hold values from -0.125 to 0.125
- down_weight: bfloat16 [8, 4096, 2048], P('ep', 'tp'), may hold values from -0.125 to 0.125
Outputs:
- mixed: bfloat16 [2048, 2048], P('ep', 'tp')
- expert_out: bfloat16 [1024, 2048], P('ep', 'tp')
Inputs may be any that keep to these rules, and one draw needn't show every extreme that they name: `routes`: within the rows of one device (aligned blocks of 128 rows) no expert is named more than 48 times, and the 2 experts of a row differ.
All inputs are finite; a program needn't handle non-finite values.
Results may differ from a plain program's by a relative error of at most 0.018.
Values may be sent and summed in bfloat16 or wider, within the bound.
A program may use at most 128 MiB of HBM per device.

v0:
```python
import functools

import jax
import jax.numpy as jnp
from jax import lax
from jax.experimental import pallas as pl
from jax.experimental.pallas import tpu as pltpu
from jax.sharding import PartitionSpec as P

norm_eps = 1e-06
rope_base = 10000.0


def rope_turn(inputs, positions):
    half_dim = inputs.shape[-1] // 2
    inverse = rope_base ** (-2.0 * jnp.arange(half_dim, dtype=jnp.float32) / inputs.shape[-1])
    angles = positions.astype(jnp.float32)[:, None] * inverse[None, :]
    cos_table = jnp.cos(angles)[:, None, None, :]
    sin_table = jnp.sin(angles)[:, None, None, :]
    first_half = inputs[..., :half_dim]
    second_half = inputs[..., half_dim:]
    return jnp.concatenate(
        [
            first_half * cos_table - second_half * sin_table,
            second_half * cos_table + first_half * sin_table,
        ],
        axis=-1,
    )


def mixer_half(query_maps, key_maps, value_rows, head_lambda, head_gain, out_weight):
    row_count = query_maps.shape[0]
    head_count = head_lambda.shape[0]
    head_dim = query_maps.shape[1] // (2 * head_count)
    value_dim = value_rows.shape[1] // head_count
    model_width = out_weight.shape[1]
    score_scale = head_dim ** (-0.5)
    offset = lax.axis_index("ep") * row_count
    positions = offset + jnp.arange(row_count, dtype=jnp.int32)
    last_row = offset + row_count - 1
    rotated_q = rope_turn(
        query_maps.astype(jnp.float32).reshape(row_count, head_count, 2, head_dim), positions
    ).astype(jnp.bfloat16)
    rotated_k = rope_turn(
        key_maps.astype(jnp.float32).reshape(row_count, head_count, 2, head_dim), positions
    ).astype(jnp.bfloat16)
    rotated_k = rotated_k.reshape(row_count, head_count * 2 * head_dim)
    initial = (
        jnp.full((head_count, 2, row_count), -1e30, jnp.float32),
        jnp.zeros((head_count, 2, row_count), jnp.float32),
        jnp.zeros((head_count, 2, row_count, value_dim), jnp.float32),
    )
    piece_k = lax.all_gather(rotated_k, "ep", axis=0, tiled=True)
    piece_v = lax.all_gather(value_rows, "ep", axis=0, tiled=True)
    piece_len = piece_k.shape[0]
    block_size = 1024

    def attend(state):

        def fold_step(inner, block_index):
            block_start = block_index * block_size
            block_k = lax.dynamic_slice_in_dim(piece_k, block_start, block_size, 0).reshape(
                block_size, head_count, 2, head_dim
            )
            block_v = lax.dynamic_slice_in_dim(piece_v, block_start, block_size, 0).reshape(
                block_size, head_count, value_dim
            )
            scores = (
                jnp.einsum(
                    "qhmd,khmd->hmqk", rotated_q, block_k, preferred_element_type=jnp.float32
                )
                * score_scale
            )
            key_pos = block_start + jnp.arange(block_size, dtype=jnp.int32)
            causal = key_pos[None, :] <= positions[:, None]
            masked = jnp.where(causal, scores, -1e30)
            run_max, run_sum, run_acc = inner
            new_max = jnp.maximum(run_max, jnp.max(masked, axis=-1))
            expd = jnp.where(causal, jnp.exp(masked - new_max[..., None]), 0.0)
            rescale = jnp.exp(run_max - new_max)
            new_sum = run_sum * rescale + jnp.sum(expd, axis=-1)
            new_acc = run_acc * rescale[..., None] + jnp.einsum(
                "hmqk,khe->hmqe",
                expd.astype(jnp.bfloat16),
                block_v,
                preferred_element_type=jnp.float32,
            )
            return ((new_max, new_sum, new_acc), None)

        result, _ = lax.scan(fold_step, state, jnp.arange(piece_len // block_size, dtype=jnp.int32))
        return result

    def skip_piece(state):
        return state

    run_max, run_sum, run_acc = lax.cond(jnp.int32(0) <= last_row, attend, skip_piece, initial)
    first_map = run_acc[:, 0] / run_sum[:, 0][..., None]
    second_map = run_acc[:, 1] / run_sum[:, 1][..., None]
    difference = first_map - head_lambda[:, None, None] * second_map
    head_out = (
        difference
        * lax.rsqrt(jnp.mean(difference * difference, axis=-1, keepdims=True) + norm_eps)
        * head_gain
    ).astype(jnp.bfloat16)
    partial_value = jnp.einsum(
        "hqe,hed->qd",
        head_out,
        out_weight.reshape(head_count, value_dim, model_width),
        preferred_element_type=jnp.float32,
    )
    return lax.psum_scatter(
        partial_value.astype(jnp.bfloat16), "tp", scatter_dimension=1, tiled=True
    )


def expert_half(
    expert_rows, expert_gain, routes, route_weights, gate_weight, up_weight, down_weight
):
    ep_count = lax.axis_size("ep")
    tp_count = lax.axis_size("tp")
    row_count, model_width = expert_rows.shape
    pick_count = routes.shape[1]
    capacity = 3 * row_count * pick_count // (2 * ep_count)
    column_count = model_width // tp_count
    inputs = expert_rows.astype(jnp.float32)
    normed = (
        inputs
        * lax.rsqrt(jnp.mean(inputs * inputs, axis=-1, keepdims=True) + norm_eps)
        * expert_gain
    ).astype(jnp.bfloat16)
    expert_ids = routes.reshape(-1)
    one_hot = (expert_ids[:, None] == jnp.arange(ep_count, dtype=jnp.int32)[None, :]).astype(
        jnp.int32
    )
    slot_index = jnp.sum((jnp.cumsum(one_hot, axis=0) - one_hot) * one_hot, axis=1)
    source_row = jnp.arange(row_count * pick_count, dtype=jnp.int32) // pick_count
    empty = jnp.zeros((ep_count, capacity, normed.shape[1]), jnp.bfloat16)
    arrived = lax.all_to_all(
        empty.at[expert_ids, slot_index].set(normed[source_row]),
        "ep",
        split_axis=0,
        concat_axis=0,
        tiled=True,
    )
    slot_count = arrived.shape[1]
    flat_rows = arrived.reshape(ep_count * slot_count, model_width)
    gate_values = jnp.dot(flat_rows, gate_weight[0], preferred_element_type=jnp.float32)
    up_values = jnp.dot(flat_rows, up_weight[0], preferred_element_type=jnp.float32)
    hidden = (jax.nn.silu(gate_values) * up_values).astype(jnp.bfloat16)
    partial_value = jnp.dot(hidden, down_weight[0], preferred_element_type=jnp.float32).reshape(
        ep_count, slot_count, model_width
    )
    summed = lax.psum_scatter(
        partial_value.astype(jnp.bfloat16), "tp", scatter_dimension=2, tiled=True
    )
    returned = lax.all_to_all(summed, "ep", split_axis=0, concat_axis=0, tiled=True)
    picked = returned[expert_ids, slot_index].reshape(row_count, pick_count, column_count)
    combined = jnp.sum(route_weights[..., None] * picked.astype(jnp.float32), axis=1)
    return combined.astype(jnp.bfloat16)


MESH = pl.DeviceIdType.MESH


def remote(source, target, send_sem, recv_sem, device):
    return pltpu.make_async_remote_copy(
        src_ref=source,
        dst_ref=target,
        send_sem=send_sem,
        recv_sem=recv_sem,
        device_id=device,
        device_id_type=MESH,
    )


def layer_kernel(
    n_ep,
    n_tp,
    rows_ref,
    norm_gain_ref,
    routes_ref,
    route_weights_ref,
    query_ref,
    key_ref,
    value_ref,
    cos_ref,
    sin_ref,
    lambda_ref,
    gain_ref,
    gate_hbm,
    up_hbm,
    down_hbm,
    weight_hbm,
    expert_ref,
    mixed_ref,
    slots_ref,
    all_ref,
    packed,
    gathered,
    gate_vmem,
    up_vmem,
    down_vmem,
    hidden,
    partial,
    arrived,
    summed,
    returned,
    weight_vmem,
    heads,
    landed,
    mixed_partial,
    mixed_arrived,
    weight_sem,
    local_sem,
    disp_send,
    disp_recv,
    gath_send,
    gath_recv,
    part_send,
    part_recv,
    ret_send,
    ret_recv,
    qkv_send,
    qkv_recv,
    pair_send,
    pair_recv,
    head_send,
    head_recv,
    mixed_send,
    mixed_recv,
):
    ep = lax.axis_index("ep")
    tp = lax.axis_index("tp")
    n_z = n_ep // 2
    z, core = ep // 2, lax.rem(ep, 2)
    capacity, width = slots_ref.shape[1:]
    rows = n_ep * capacity
    head_width = packed.shape[2] // 3
    half = head_width // 2
    weights = [
        pltpu.make_async_copy(gate_hbm, gate_vmem, weight_sem.at[0]),
        pltpu.make_async_copy(up_hbm, up_vmem, weight_sem.at[1]),
        pltpu.make_async_copy(down_hbm, down_vmem, weight_sem.at[2]),
        pltpu.make_async_copy(weight_hbm, weight_vmem, weight_sem.at[3]),
    ]
    for copy in weights:
        copy.start()
    peers = [{"ep": lax.rem(ep + d, n_ep)} for d in range(1, n_ep)]
    peers += [{"tp": lax.rem(tp + d, n_tp)} for d in range(1, n_tp)]
    barrier = pltpu.get_barrier_semaphore()
    for device in peers:
        pl.semaphore_signal(barrier, inc=1, device_id=device, device_id_type=MESH)

    token_count = rows_ref.shape[0]
    picks = routes_ref.shape[0]
    entries = rows_ref[...].astype(jnp.float32)
    inverse_norm = lax.rsqrt(jnp.mean(entries * entries, axis=1, keepdims=True) + norm_eps)
    own = pl.ds(pl.multiple_of(tp * width, width), width)
    normed = rows_ref[:, own].astype(jnp.float32) * inverse_norm * norm_gain_ref[:, own]
    normed = normed.astype(jnp.bfloat16)
    named_rows = -(-n_ep // 16) * 16
    label = lax.broadcasted_iota(jnp.int32, (named_rows, token_count), 0)
    named = [
        jnp.where(label == routes_ref[k : k + 1, :], 1.0, 0.0).astype(jnp.float32)
        for k in range(picks)
    ]
    before = lax.broadcasted_iota(jnp.int32, (token_count, token_count), 0)
    after = lax.broadcasted_iota(jnp.int32, (token_count, token_count), 1)
    earlier = jnp.dot(
        sum(named).astype(jnp.bfloat16),
        jnp.where(before < after, 1.0, 0.0).astype(jnp.bfloat16),
        preferred_element_type=jnp.float32,
    )
    slot_of = lax.broadcasted_iota(jnp.int32, (rows, token_count), 0)
    select = []
    for k in range(picks):
        rank = jnp.sum(named[k] * earlier, axis=0, keepdims=True).astype(jnp.int32)
        place = routes_ref[k : k + 1, :] * capacity + rank
        select.append(jnp.where(slot_of == place, 1.0, 0.0).astype(jnp.float32))
    slots_ref[...] = (
        jnp.dot(
            sum(select).astype(jnp.bfloat16), normed, preferred_element_type=jnp.float32
        )
        .astype(jnp.bfloat16)
        .reshape(n_ep, capacity, width)
    )
    pl.semaphore_wait(barrier, len(peers))
    mine = tp * n_ep + ep
    dispatch = [pltpu.make_async_copy(slots_ref.at[ep], gathered.at[mine], local_sem.at[0])]
    for d in range(1, n_ep):
        target = lax.rem(ep + d, n_ep)
        dispatch.append(
            remote(
                slots_ref.at[target],
                gathered.at[mine],
                disp_send.at[d],
                disp_recv.at[d],
                {"ep": target},
            )
        )
    for copy in dispatch:
        copy.start()

    for head in range(n_z):
        for index, ref in ((0, query_ref), (1, key_ref)):
            for m in range(2):
                at = head * head_width + m * half
                entry = ref[:, at : at + half].astype(jnp.float32)
                turned = entry * cos_ref[...] + pltpu.roll(entry, half // 2, 1) * sin_ref[...]
                to = index * head_width + m * half
                packed[head, :, to : to + half] = turned.astype(jnp.bfloat16)
        packed[head, :, 2 * head_width :] = value_ref[
            :, head * head_width : (head + 1) * head_width
        ]
    exchange = [pltpu.make_async_copy(packed.at[z], all_ref.at[ep], qkv_recv.at[z])]
    upper = (2 * z) // n_z
    for turn in range(n_z - 1):
        far = n_z - 1 - turn
        falling = far - (z - far + n_z) // n_z
        rising = turn + (turn - z + n_z) // n_z
        target = falling * (1 - upper) + rising * upper
        exchange.append(
            remote(
                packed.at[target],
                all_ref.at[ep],
                qkv_send.at[turn],
                qkv_recv.at[z],
                {"ep": 2 * target + core},
            )
        )
    for copy in exchange:
        copy.start()

    spread = []
    for d in range(n_ep):
        source = lax.rem(ep + n_ep - d, n_ep)
        if d == 0:
            dispatch[0].wait()
        else:
            dispatch[d].wait_recv()
        slot = gathered.at[tp * n_ep + source]
        for t in range(1, n_tp):
            copy = remote(
                slot,
                slot,
                gath_send.at[d * n_tp + t],
                gath_recv.at[d * n_tp + t],
                {"tp": lax.rem(tp + t, n_tp)},
            )
            copy.start()
            spread.append(copy)
    for copy in spread:
        copy.wait_recv()
    weights[0].wait()
    weights[1].wait()
    tile = 256

    def hidden_tile(j, carry):
        columns = pl.ds(pl.multiple_of(j * tile, tile), tile)
        gate = jnp.zeros((rows, tile), jnp.float32)
        up = jnp.zeros((rows, tile), jnp.float32)
        for i in range(n_tp):
            block = gathered[i * n_ep : (i + 1) * n_ep].reshape(rows, width)
            gate += jnp.dot(
                block,
                gate_vmem[0, i * width : (i + 1) * width, columns],
                preferred_element_type=jnp.float32,
            )
            up += jnp.dot(
                block,
                up_vmem[0, i * width : (i + 1) * width, columns],
                preferred_element_type=jnp.float32,
            )
        hidden[:, columns] = (gate / (1.0 + jnp.exp(-gate)) * up).astype(jnp.bfloat16)
        return carry

    lax.fori_loop(0, hidden.shape[1] // tile, hidden_tile, 0)
    weights[2].wait()
    scatter = []
    for d in list(range(1, n_tp)) + [0]:
        target = lax.rem(tp + d, n_tp)
        columns = pl.ds(pl.multiple_of(target * width, width), width)
        partial[d] = jnp.dot(
            hidden[...], down_vmem[0, :, columns], preferred_element_type=jnp.float32
        ).astype(jnp.bfloat16)
        if d:
            copy = remote(
                partial.at[d], arrived.at[d], part_send.at[d], part_recv.at[d], {"tp": target}
            )
            copy.start()
            scatter.append(copy)
    pairs = []

    def pass_on(source):
        landing = all_ref.at[2 * source + core]
        pltpu.make_async_copy(packed.at[source], landing, qkv_recv.at[source]).wait()
        part = all_ref.at[2 * source + core, :, pl.ds(head_width, 2 * head_width)]
        copy = remote(
            part, part, pair_send.at[source], pair_recv.at[source], {"ep": ep + 1 - 2 * core}
        )
        copy.start()
        pairs.append(copy)

    row_count = all_ref.shape[1]
    value_width = head_width
    head_weight = jnp.sum(
        jnp.where(lax.broadcasted_iota(jnp.int32, lambda_ref.shape, 1) == z, lambda_ref[...], 0.0),
        axis=1,
        keepdims=True,
    )
    scale = half ** (-0.5)
    pair_rows = 2 * row_count
    row = lax.broadcasted_iota(jnp.int32, (row_count, pair_rows), 0) + core * row_count
    causal = lax.broadcasted_iota(jnp.int32, (row_count, pair_rows), 1) <= row

    def sender(block):
        return remote(
            heads.at[block],
            landed.at[z],
            head_send.at[block],
            head_recv.at[z],
            {"ep": 2 * block + core},
        )

    def keeper(block):
        return pltpu.make_async_copy(heads.at[block], landed.at[block], head_recv.at[block])

    def attend(block):
        maps = []
        for m in range(2):
            query = all_ref[2 * block + core, :, m * half : (m + 1) * half]
            pieces = []
            for pair in range(block + 1):
                at = value_width + m * half
                keys = all_ref[2 * pair : 2 * pair + 2, :, at : at + half].reshape(pair_rows, half)
                scores = lax.dot_general(
                    query, keys, (((1,), (1,)), ((), ())), preferred_element_type=jnp.float32
                )
                scores = scores * scale
                if pair == block:
                    scores = jnp.where(causal, scores, -1e30)
                pieces.append(scores)
            peak = functools.reduce(
                jnp.maximum, [jnp.max(piece, axis=1, keepdims=True) for piece in pieces]
            )
            total = jnp.zeros((row_count, 1), jnp.float32)
            outcome = jnp.zeros((row_count, value_width), jnp.float32)
            for pair in range(block + 1):
                expd = jnp.exp(pieces[pair] - peak)
                total += jnp.sum(expd, axis=1, keepdims=True)
                values = all_ref[2 * pair : 2 * pair + 2, :, 2 * value_width :].reshape(
                    pair_rows, value_width
                )
                outcome += jnp.dot(
                    expd.astype(jnp.bfloat16), values, preferred_element_type=jnp.float32
                )
            maps.append(outcome / total)
        difference = maps[0] - head_weight * maps[1]
        mean = jnp.mean(difference * difference, axis=1, keepdims=True)
        heads[block] = (difference * lax.rsqrt(mean + norm_eps) * gain_ref[...]).astype(
            jnp.bfloat16
        )

        @pl.when(z == block)
        def _():
            keeper(block).start()

        @pl.when(z != block)
        def _():
            sender(block).start()

    pass_on(0)
    for block in range(n_z):
        if len(pairs) <= block or 1 <= block + 1 < n_z - 1:
            pass_on(len(pairs))
        pairs[block].wait_recv()
        attend(block)
    total = partial[0].astype(jnp.float32)
    for d in range(1, n_tp):
        scatter[d - 1].wait_recv()
        total += arrived[d].astype(jnp.float32)
    summed[...] = total.astype(jnp.bfloat16).reshape(n_ep, capacity, width)
    back = [pltpu.make_async_copy(summed.at[ep], returned.at[ep], local_sem.at[2])]
    for d in range(1, n_ep):
        target = lax.rem(ep + d, n_ep)
        back.append(
            remote(
                summed.at[target],
                returned.at[ep],
                ret_send.at[d],
                ret_recv.at[d],
                {"ep": target},
            )
        )
    for copy in back:
        copy.start()

    for block in range(n_z):
        keeper(block).wait()
    weights[3].wait()
    mixed_scatter = []
    for d in list(range(1, n_tp)) + [0]:
        target = lax.rem(tp + d, n_tp)
        columns = pl.ds(pl.multiple_of(target * width, width), width)
        product = jnp.zeros((row_count, width), jnp.float32)
        for h in range(n_z):
            product += jnp.dot(
                landed[h],
                weight_vmem[h * value_width : (h + 1) * value_width, columns],
                preferred_element_type=jnp.float32,
            )
        mixed_partial[d] = product.astype(jnp.bfloat16)
        if d:
            copy = remote(
                mixed_partial.at[d], mixed_arrived.at[d], mixed_send.at[d], mixed_recv.at[d], {"tp": target}
            )
            copy.start()
            mixed_scatter.append(copy)
    back[0].wait()
    for copy in back[1:]:
        copy.wait_recv()
    flat = returned[...].reshape(rows, width)
    result = jnp.zeros(expert_ref.shape, jnp.float32)
    for k in range(picks):
        picked = lax.dot_general(
            select[k].astype(jnp.bfloat16),
            flat,
            (((0,), (0,)), ((), ())),
            preferred_element_type=jnp.float32,
        )
        spread_out = jnp.where(before == after, route_weights_ref[k : k + 1, :], 0.0)
        result += jnp.sum(spread_out, axis=1, keepdims=True) * picked
    expert_ref[...] = result.astype(expert_ref.dtype)
    total = mixed_partial[0].astype(jnp.float32)
    for d in range(1, n_tp):
        mixed_scatter[d - 1].wait_recv()
        total += mixed_arrived[d].astype(jnp.float32)
    mixed_ref[...] = total.astype(jnp.bfloat16)
    for copy in mixed_scatter:
        copy.wait_send()
    for block in range(n_z):

        @pl.when(z != block)
        def _():
            sender(block).wait_send()
    for copy in dispatch[1:] + exchange[1:] + spread + scatter + back[1:] + pairs:
        copy.wait_send()


def fused(
    query_maps,
    key_maps,
    value_rows,
    head_lambda,
    head_gain,
    out_weight,
    expert_rows,
    expert_gain,
    routes,
    route_weights,
    gate_weight,
    up_weight,
    down_weight,
):
    n_ep = lax.axis_size("ep")
    n_tp = lax.axis_size("tp")
    n_z = n_ep // 2
    ep = lax.axis_index("ep")
    row_count = query_maps.shape[0]
    head_width = query_maps.shape[1] // n_z
    head_dim = head_width // 2
    token_count, model_width = expert_rows.shape
    capacity = 3 * token_count * routes.shape[1] // (2 * n_ep)
    width = model_width // n_tp
    hidden_width = gate_weight.shape[2]
    slot_rows = n_ep * capacity

    positions = ep * row_count + jnp.arange(row_count, dtype=jnp.int32)
    half_dim = head_dim // 2
    inverse = rope_base ** (-2.0 * jnp.arange(half_dim, dtype=jnp.float32) / head_dim)
    angles = positions.astype(jnp.float32)[:, None] * inverse[None, :]
    cosine, sine = jnp.cos(angles), jnp.sin(angles)
    cos_table = jnp.concatenate([cosine, cosine], axis=1)
    sin_table = jnp.concatenate([-sine, sine], axis=1)

    vmem = pl.BlockSpec(memory_space=pltpu.VMEM)
    hbm = pl.BlockSpec(memory_space=pl.ANY)
    dma = pltpu.SemaphoreType.DMA
    bf16 = jnp.bfloat16
    expert_out, mixed = pl.pallas_call(
        functools.partial(layer_kernel, n_ep, n_tp),
        out_shape=(
            jax.ShapeDtypeStruct((token_count, width), bf16),
            jax.ShapeDtypeStruct((row_count, width), bf16),
        ),
        in_specs=[vmem] * 11 + [hbm] * 4,
        out_specs=(vmem, vmem),
        scratch_shapes=[
            pltpu.VMEM((n_ep, capacity, width), bf16),
            pltpu.VMEM((n_ep, row_count, 3 * head_width), bf16),
            pltpu.VMEM((n_z, row_count, 3 * head_width), bf16),
            pltpu.VMEM((n_tp * n_ep, capacity, width), bf16),
            pltpu.VMEM(gate_weight.shape, bf16),
            pltpu.VMEM(up_weight.shape, bf16),
            pltpu.VMEM(down_weight.shape, bf16),
            pltpu.VMEM((slot_rows, hidden_width), bf16),
            pltpu.VMEM((n_tp, slot_rows, width), bf16),
            pltpu.VMEM((n_tp, slot_rows, width), bf16),
            pltpu.VMEM((n_ep, capacity, width), bf16),
            pltpu.VMEM((n_ep, capacity, width), bf16),
            pltpu.VMEM(out_weight.shape, bf16),
            pltpu.VMEM((n_z, row_count, head_width), bf16),
            pltpu.VMEM((n_z, row_count, head_width), bf16),
            pltpu.VMEM((n_tp, row_count, width), bf16),
            pltpu.VMEM((n_tp, row_count, width), bf16),
            dma((4,)),
            dma((3,)),
            dma((n_ep,)),
            dma((n_ep,)),
            dma((n_ep * n_tp,)),
            dma((n_ep * n_tp,)),
            dma((n_tp,)),
            dma((n_tp,)),
            dma((n_ep,)),
            dma((n_ep,)),
            dma((n_z,)),
            dma((n_z,)),
            dma((n_z,)),
            dma((n_z,)),
            dma((n_z,)),
            dma((n_z,)),
            dma((n_tp,)),
            dma((n_tp,)),
        ],
        compiler_params=pltpu.CompilerParams(
            collective_id=0, has_side_effects=True, vmem_limit_bytes=60 * 1024 * 1024
        ),
        name="layer",
    )(
        expert_rows,
        expert_gain.reshape(1, model_width),
        routes.T,
        route_weights.T,
        query_maps,
        key_maps,
        value_rows,
        cos_table,
        sin_table,
        head_lambda.reshape(1, n_z),
        head_gain.reshape(1, head_width),
        gate_weight,
        up_weight,
        down_weight,
        out_weight,
    )
    return (mixed, expert_out)


def on_device(
    query_maps,
    key_maps,
    value_rows,
    head_lambda,
    head_gain,
    out_weight,
    expert_rows,
    expert_gain,
    routes,
    route_weights,
    gate_weight,
    up_weight,
    down_weight,
):
    n_ep = lax.axis_size("ep")
    head_count = head_lambda.shape[0]
    capacity = 3 * expert_rows.shape[0] * routes.shape[1] // (2 * n_ep)
    if (
        2 * head_count == n_ep
        and capacity % 16 == 0
        and value_rows.shape[1] == query_maps.shape[1] == 256 * head_count
    ):
        return fused(
            query_maps,
            key_maps,
            value_rows,
            head_lambda,
            head_gain,
            out_weight,
            expert_rows,
            expert_gain,
            routes,
            route_weights,
            gate_weight,
            up_weight,
            down_weight,
        )
    mixed = mixer_half(query_maps, key_maps, value_rows, head_lambda, head_gain, out_weight)
    expert_out = expert_half(
        expert_rows, expert_gain, routes, route_weights, gate_weight, up_weight, down_weight
    )
    return (mixed, expert_out)


def solution(mesh):
    placed = (
        P("ep", "tp"),
        P("ep", "tp"),
        P("ep", "tp"),
        P("tp"),
        P(),
        P("tp", None),
        P("ep", None),
        P(),
        P("ep", None),
        P("ep", None),
        P("ep", None, "tp"),
        P("ep", None, "tp"),
        P("ep", "tp", None),
    )
    return jax.shard_map(
        on_device,
        mesh=mesh,
        in_specs=placed,
        out_specs=(P("ep", "tp"), P("ep", "tp")),
        check_vma=False,
    )
```

profile of v0, /device:TPU:25, one launch (start us, length us, event | category | flops | bytes accessed | tf_op | source)
XLA Modules:
  0.0 89.6 jit_solution(15566822173114283555)
XLA Ops:
  0.7 0.5 fusion
  1.2 0.8 pad_maximum_fusion
  2.0 84.3 %layer.1 = (bf16[128,512]{1,0:T(8,128)(2,1)}, bf16[256,512]{1,0:T(8,128)(2,1)}) custom-call(bf16[128,2048]{1,0:T(8,128)(2,1)} %rows_ref.1, f32[1,2048]{1,0:T(1,128)} %bitcast.5, s32[2,128]{1,0:T(2,128)} %bitcast.6, f32[2,128]{1,0:T(2,128)} %bitcast.7, bf16[256,1024]{1,0:T(8,128)(2,1)} %query_ref.1, bf16[256,1024]{1,0:T(8,128)(2,1)} %key_ref.1, ...), custom_call_target="tpu_custom_call" | custom-call | tf_op jit(solution)/shard_map/layer/pallas_call | solution.py:590
  86.4 1.7 %copy.17 = bf16[256,512]{1,0:T(8,128)(2,1)} copy(bf16[256,512]{1,0:T(8,128)(2,1)} %get-tuple-element.13) | data formatting | bytes 524288
  88.1 1.6 %copy.18 = bf16[128,512]{1,0:T(8,128)(2,1)} copy(bf16[128,512]{1,0:T(8,128)(2,1)} %get-tuple-element.14) | data formatting | bytes 262144
  (2 shorter events, 0.0 us)
where the time goes:
time: 89.8 us; the launch traced here: 89.6 us
  Pallas kernels  84.3 us (94%)
  local copies, waits for them, and re-layouts  3.24 us (4%)
  other arithmetic  1.39 us (2%)
    pallas_call x1, Pallas kernels, fused(): pl.pallas_call(functools.partial(layer_kernel, n_ep, n_tp), out_shape=(ja...  84.3 us
    unnamed x2, local copies, waits for them, and re-layouts  3.24 us

commit v1 on v0

--- a/solution.py
+++ b/solution.py
@@ -194,8 +194,22 @@
     expert_ref,
     mixed_ref,
     slots_ref,
-    all_ref,
-    packed,
+    packed_q,
+    packed_kv,
+    own_q,
+    own_kv,
+    below_kv,
+    lower_kv,
+    upper_q,
+    own_stat,
+    upper_stat,
+    low_stat,
+    back_stat,
+    own_maps,
+    own_part,
+    own_diff,
+    low_part,
+    low_diff,
     gathered,
     gate_vmem,
     up_vmem,
@@ -207,7 +221,6 @@
     returned,
     weight_vmem,
     heads,
-    landed,
     mixed_partial,
     mixed_arrived,
     weight_sem,
@@ -220,23 +233,41 @@
     part_recv,
     ret_send,
     ret_recv,
-    qkv_send,
-    qkv_recv,
-    pair_send,
-    pair_recv,
-    head_send,
-    head_recv,
+    swap_send,
+    swap_recv,
+    below_send,
+    below_recv,
+    lower_send,
+    lower_recv,
+    upper_send,
+    upper_recv,
+    stat_send,
+    stat_recv,
+    back_send,
+    back_recv,
+    diff_send,
+    diff_recv,
+    cross_send,
+    cross_recv,
     mixed_send,
     mixed_recv,
 ):
     ep = lax.axis_index("ep")
     tp = lax.axis_index("tp")
     n_z = n_ep // 2
+    middle = n_z // 2
     z, core = ep // 2, lax.rem(ep, 2)
+    odd = lax.rem(z, 2)
+    asks = [z >= middle, odd == 1]
+    host = [middle - 1, z - 1]
+    seat = [lax.rem(z, middle), 0]
+    partner = {"ep": ep + 1 - 2 * core}
     capacity, width = slots_ref.shape[1:]
     rows = n_ep * capacity
-    head_width = packed.shape[2] // 3
+    head_count, row_count, head_width = packed_q.shape
+    share = head_count // 2
     half = head_width // 2
+    first = core * share
     weights = [
         pltpu.make_async_copy(gate_hbm, gate_vmem, weight_sem.at[0]),
         pltpu.make_async_copy(up_hbm, up_vmem, weight_sem.at[1]),
@@ -284,7 +315,8 @@
         .astype(jnp.bfloat16)
         .reshape(n_ep, capacity, width)
     )
-    pl.semaphore_wait(barrier, len(peers))
+    with jax.named_scope("barrier"):
+        pl.semaphore_wait(barrier, len(peers))
     mine = tp * n_ep + ep
     dispatch = [pltpu.make_async_copy(slots_ref.at[ep], gathered.at[mine], local_sem.at[0])]
     for d in range(1, n_ep):
@@ -301,56 +333,299 @@
     for copy in dispatch:
         copy.start()
 
-    for head in range(n_z):
-        for index, ref in ((0, query_ref), (1, key_ref)):
-            for m in range(2):
-                at = head * head_width + m * half
+    for head in range(head_count):
+        for m in range(2):
+            at = head * head_width + m * half
+            to = slice(m * half, (m + 1) * half)
+            for ref, packed in ((query_ref, packed_q), (key_ref, packed_kv)):
                 entry = ref[:, at : at + half].astype(jnp.float32)
                 turned = entry * cos_ref[...] + pltpu.roll(entry, half // 2, 1) * sin_ref[...]
-                to = index * head_width + m * half
-                packed[head, :, to : to + half] = turned.astype(jnp.bfloat16)
-        packed[head, :, 2 * head_width :] = value_ref[
+                packed[head, :, to] = turned.astype(jnp.bfloat16)
+        packed_kv[head, :, head_width:] = value_ref[
             :, head * head_width : (head + 1) * head_width
         ]
-    exchange = [pltpu.make_async_copy(packed.at[z], all_ref.at[ep], qkv_recv.at[z])]
-    upper = (2 * z) // n_z
-    for turn in range(n_z - 1):
-        far = n_z - 1 - turn
-        falling = far - (z - far + n_z) // n_z
-        rising = turn + (turn - z + n_z) // n_z
-        target = falling * (1 - upper) + rising * upper
-        exchange.append(
+    other = share - first
+    swaps = []
+    for j in range(share):
+        swaps += [
             remote(
-                packed.at[target],
-                all_ref.at[ep],
-                qkv_send.at[turn],
-                qkv_recv.at[z],
-                {"ep": 2 * target + core},
-            )
-        )
-    for copy in exchange:
+                packed_q.at[other + j],
+                own_q.at[j, core],
+                swap_send.at[0, j],
+                swap_recv.at[0, j],
+                partner,
+            ),
+            remote(
+                packed_kv.at[other + j],
+                own_kv.at[j, core],
+                swap_send.at[1, j],
+                swap_recv.at[1, j],
+                partner,
+            ),
+        ]
+    keeps = []
+    for j in range(share):
+        keeps += [
+            pltpu.make_async_copy(packed_q.at[first + j], own_q.at[j, core], local_sem.at[3 + j]),
+            pltpu.make_async_copy(
+                packed_kv.at[first + j], own_kv.at[j, core], local_sem.at[3 + share + j]
+            ),
+        ]
+    for copy in swaps + keeps:
         copy.start()
 
+    def lift(side):
+        return remote(
+            packed_kv.at[side * share],
+            below_kv.at[0, core],
+            below_send.at[side],
+            below_recv.at[core],
+            {"ep": lax.rem(ep - core + 2 + side, n_ep)},
+        )
+
+    def lift_far(side):
+        return remote(
+            packed_kv.at[side * share + 1],
+            lower_kv.at[0, 2 * lax.rem(z, middle) + core],
+            lower_send.at[side],
+            lower_recv.at[2 * lax.rem(z, middle) + core],
+            {"ep": 2 * middle + side},
+        )
+
+    def ask(side, j):
+        return remote(
+            packed_q.at[side * share + j],
+            upper_q.at[seat[j], core],
+            upper_send.at[side, j],
+            upper_recv.at[seat[j], core],
+            {"ep": 2 * host[j] + side},
+        )
+
+    def wait_landed(ref, sem):
+        pltpu.make_async_copy(ref, ref, sem).wait()
+
     spread = []
-    for d in range(n_ep):
-        source = lax.rem(ep + n_ep - d, n_ep)
-        if d == 0:
-            dispatch[0].wait()
-        else:
-            dispatch[d].wait_recv()
-        slot = gathered.at[tp * n_ep + source]
-        for t in range(1, n_tp):
-            copy = remote(
-                slot,
-                slot,
-                gath_send.at[d * n_tp + t],
-                gath_recv.at[d * n_tp + t],
-                {"tp": lax.rem(tp + t, n_tp)},
-            )
-            copy.start()
-            spread.append(copy)
-    for copy in spread:
-        copy.wait_recv()
+    with jax.named_scope("wait_disp"):
+        for d in range(n_ep):
+            source = lax.rem(ep + n_ep - d, n_ep)
+            if d == 0:
+                dispatch[0].wait()
+            else:
+                dispatch[d].wait_recv()
+            slot = gathered.at[tp * n_ep + source]
+            for t in range(1, n_tp):
+                copy = remote(
+                    slot,
+                    slot,
+                    gath_send.at[d * n_tp + t],
+                    gath_recv.at[d * n_tp + t],
+                    {"tp": lax.rem(tp + t, n_tp)},
+                )
+                copy.start()
+                spread.append(copy)
+
+    for j in range(share):
+        for side in range(2):
+
+            @pl.when(asks[j])
+            def _():
+                ask(side, j).start()
+
+    for side in range(2):
+
+        @pl.when(odd == 0)
+        def _():
+            lift(side).start()
+
+    for side in range(2):
+
+        @pl.when(z < middle)
+        def _():
+            lift_far(side).start()
+
+    row = lax.broadcasted_iota(jnp.int32, (row_count, row_count), 0)
+    column = lax.broadcasted_iota(jnp.int32, (row_count, row_count), 1)
+    causal = column <= row
+    wide = lax.broadcasted_iota(jnp.int32, (row_count, 2 * row_count), 0) + row_count
+    wide_causal = lax.broadcasted_iota(jnp.int32, (row_count, 2 * row_count), 1) <= wide
+    diagonal = column == row
+    scale = half ** (-0.5)
+    stat_row = lax.broadcasted_iota(jnp.int32, (8, row_count), 0)
+
+    def as_column(values):
+        return jnp.sum(jnp.where(diagonal, values, 0.0), axis=1, keepdims=True)
+
+    def as_row(values):
+        return jnp.sum(jnp.where(diagonal, values, 0.0), axis=0, keepdims=True)
+
+    def as_stats(levels):
+        return jnp.where(stat_row == 0, as_row(levels[0]), as_row(levels[1]))
+
+    def head_weight(j):
+        lanes = lax.broadcasted_iota(jnp.int32, lambda_ref.shape, 1)
+        return jnp.sum(
+            jnp.where(lanes == first + j, lambda_ref[...], 0.0), axis=1, keepdims=True
+        )
+
+    def fold(query_of, pieces, m):
+        scores = []
+        for keys_of, values_of, mask in pieces:
+            piece = lax.dot_general(
+                query_of(m), keys_of(m), (((1,), (1,)), ((), ())), preferred_element_type=jnp.float32
+            )
+            piece = piece * scale
+            if mask is not None:
+                piece = jnp.where(mask, piece, -1e30)
+            scores.append(piece)
+        peak = functools.reduce(
+            jnp.maximum, [jnp.max(piece, axis=1, keepdims=True) for piece in scores]
+        )
+        total = jnp.zeros((row_count, 1), jnp.float32)
+        outcome = jnp.zeros((row_count, head_width), jnp.float32)
+        for piece, (keys_of, values_of, mask) in zip(scores, pieces):
+            expd = jnp.exp(piece - peak)
+            total += jnp.sum(expd, axis=1, keepdims=True)
+            outcome += jnp.dot(
+                expd.astype(jnp.bfloat16), values_of(), preferred_element_type=jnp.float32
+            )
+        return peak, total, outcome
+
+    def piece_of(ref, j, count, mask):
+        def keys_of(m):
+            keys = ref[j, :count, :, m * half : (m + 1) * half]
+            return keys.reshape(count * row_count, half)
+
+        def values_of():
+            return ref[j, :count, :, head_width:].reshape(count * row_count, head_width)
+
+        return keys_of, values_of, mask
+
+    def keep_diff(j, block, difference):
+        @pl.when(core == block)
+        def _():
+            own_diff[first + j] = difference.astype(jnp.bfloat16)
+
+        @pl.when(core != block)
+        def _():
+            own_part[j] = difference.astype(jnp.bfloat16)
+            send_diff(j).start()
+
+    def send_diff(j):
+        return remote(
+            own_part.at[j], own_diff.at[first + j], diff_send.at[j], diff_recv.at[first + j], partner
+        )
+
+    def send_stat(j):
+        return remote(
+            own_stat.at[j],
+            upper_stat.at[seat[j]],
+            stat_send.at[j],
+            stat_recv.at[seat[j]],
+            {"ep": 2 * host[j] + core},
+        )
+
+    def local_head(j, pieces):
+        swaps[2 * j].wait_recv()
+        swaps[2 * j + 1].wait_recv()
+        keeps[2 * j].wait()
+        keeps[2 * j + 1].wait()
+        for block in range(2):
+            mask = wide_causal if block else causal
+            parts = pieces + [piece_of(own_kv, j, block + 1, mask)]
+            maps, levels = [], []
+            for m in range(2):
+                peak, total, outcome = fold(
+                    lambda m: own_q[j, block, :, m * half : (m + 1) * half], parts, m
+                )
+                maps.append(outcome / total)
+                levels.append(peak + jnp.log(total))
+
+            @pl.when(asks[j])
+            def _():
+                own_maps[j, block, 0] = maps[0]
+                own_maps[j, block, 1] = maps[1]
+                own_stat[j, block] = as_stats(levels)
+
+            @pl.when(jnp.logical_not(asks[j]))
+            def _():
+                keep_diff(j, block, maps[0] - head_weight(j) * maps[1])
+
+        @pl.when(asks[j])
+        def _():
+            send_stat(j).start()
+
+    def send_cross(up, j, block, target):
+        return remote(
+            low_part.at[up, block],
+            low_diff.at[first + j],
+            cross_send.at[up, block],
+            cross_recv.at[first + j],
+            {"ep": 2 * target + block},
+        )
+
+    def send_back(up, j, block, target):
+        return remote(
+            low_stat.at[up, block],
+            back_stat.at[j, block],
+            back_send.at[up, block],
+            back_recv.at[j, block],
+            {"ep": 2 * target + core},
+        )
+
+    def cross_head(j, count, base, pieces):
+        def step(index, carry):
+            up, block = index // 2, lax.rem(index, 2)
+            target = base + up
+            wait_landed(upper_q.at[up, block], upper_recv.at[up, block])
+
+            @pl.when(block == 0)
+            def _():
+                wait_landed(upper_stat.at[up], stat_recv.at[up])
+
+            maps, levels = [], []
+            for m in range(2):
+                peak, total, outcome = fold(
+                    lambda m: upper_q[up, block, :, m * half : (m + 1) * half], pieces, m
+                )
+                level = peak + jnp.log(total)
+                above = as_column(upper_stat[up, block, m : m + 1, :])
+                whole = jnp.maximum(level, above) + jnp.log(1.0 + jnp.exp(-jnp.abs(level - above)))
+                maps.append(outcome * jnp.exp(peak - whole))
+                levels.append(level)
+            low_stat[up, block] = as_stats(levels)
+            send_back(up, j, block, target).start()
+            low_part[up, block] = (maps[0] - head_weight(j) * maps[1]).astype(jnp.bfloat16)
+            send_cross(up, j, block, target).start()
+            return carry
+
+        lax.fori_loop(0, 2 * count, step, 0)
+
+    def finish_upper(j):
+        for block in range(2):
+            wait_landed(back_stat.at[j, block], back_recv.at[j, block])
+            maps = []
+            for m in range(2):
+                below = as_column(back_stat[j, block, m : m + 1, :])
+                level = as_column(own_stat[j, block, m : m + 1, :])
+                maps.append(own_maps[j, block, m] / (1.0 + jnp.exp(below - level)))
+            keep_diff(j, block, maps[0] - head_weight(j) * maps[1])
+
+    below_piece = piece_of(below_kv, 0, 2, None)
+    lower_piece = piece_of(lower_kv, 0, 2 * middle, None)
+
+    @pl.when(z != middle)
+    def _():
+        with jax.named_scope("own1"):
+            local_head(1, [])
+
+    @pl.when(odd == 0)
+    def _():
+        with jax.named_scope("own0"):
+            local_head(0, [])
+
+    with jax.named_scope("wait_gath"):
+        for copy in spread:
+            copy.wait_recv()
     weights[0].wait()
     weights[1].wait()
     tile = 256
@@ -374,111 +649,66 @@
         hidden[:, columns] = (gate / (1.0 + jnp.exp(-gate)) * up).astype(jnp.bfloat16)
         return carry
 
-    lax.fori_loop(0, hidden.shape[1] // tile, hidden_tile, 0)
+    with jax.named_scope("gateup"):
+        lax.fori_loop(0, hidden.shape[1] // tile, hidden_tile, 0)
     weights[2].wait()
     scatter = []
-    for d in list(range(1, n_tp)) + [0]:
-        target = lax.rem(tp + d, n_tp)
-        columns = pl.ds(pl.multiple_of(target * width, width), width)
-        partial[d] = jnp.dot(
-            hidden[...], down_vmem[0, :, columns], preferred_element_type=jnp.float32
-        ).astype(jnp.bfloat16)
-        if d:
-            copy = remote(
-                partial.at[d], arrived.at[d], part_send.at[d], part_recv.at[d], {"tp": target}
-            )
-            copy.start()
-            scatter.append(copy)
-    pairs = []
-
-    def pass_on(source):
-        landing = all_ref.at[2 * source + core]
-        pltpu.make_async_copy(packed.at[source], landing, qkv_recv.at[source]).wait()
-        part = all_ref.at[2 * source + core, :, pl.ds(head_width, 2 * head_width)]
-        copy = remote(
-            part, part, pair_send.at[source], pair_recv.at[source], {"ep": ep + 1 - 2 * core}
-        )
-        copy.start()
-        pairs.append(copy)
-
-    row_count = all_ref.shape[1]
-    value_width = head_width
-    head_weight = jnp.sum(
-        jnp.where(lax.broadcasted_iota(jnp.int32, lambda_ref.shape, 1) == z, lambda_ref[...], 0.0),
-        axis=1,
-        keepdims=True,
-    )
-    scale = half ** (-0.5)
-    pair_rows = 2 * row_count
-    row = lax.broadcasted_iota(jnp.int32, (row_count, pair_rows), 0) + core * row_count
-    causal = lax.broadcasted_iota(jnp.int32, (row_count, pair_rows), 1) <= row
-
-    def sender(block):
-        return remote(
-            heads.at[block],
-            landed.at[z],
-            head_send.at[block],
-            head_recv.at[z],
-            {"ep": 2 * block + core},
-        )
-
-    def keeper(block):
-        return pltpu.make_async_copy(heads.at[block], landed.at[block], head_recv.at[block])
-
-    def attend(block):
-        maps = []
-        for m in range(2):
-            query = all_ref[2 * block + core, :, m * half : (m + 1) * half]
-            pieces = []
-            for pair in range(block + 1):
-                at = value_width + m * half
-                keys = all_ref[2 * pair : 2 * pair + 2, :, at : at + half].reshape(pair_rows, half)
-                scores = lax.dot_general(
-                    query, keys, (((1,), (1,)), ((), ())), preferred_element_type=jnp.float32
+    with jax.named_scope("down"):
+        for d in list(range(1, n_tp)) + [0]:
+            target = lax.rem(tp + d, n_tp)
+            columns = pl.ds(pl.multiple_of(target * width, width), width)
+            partial[d] = jnp.dot(
+                hidden[...], down_vmem[0, :, columns], preferred_element_type=jnp.float32
+            ).astype(jnp.bfloat16)
+            if d:
+                copy = remote(
+                    partial.at[d], arrived.at[d], part_send.at[d], part_recv.at[d], {"tp": target}
                 )
-                scores = scores * scale
-                if pair == block:
-                    scores = jnp.where(causal, scores, -1e30)
-                pieces.append(scores)
-            peak = functools.reduce(
-                jnp.maximum, [jnp.max(piece, axis=1, keepdims=True) for piece in pieces]
-            )
-            total = jnp.zeros((row_count, 1), jnp.float32)
-            outcome = jnp.zeros((row_count, value_width), jnp.float32)
-            for pair in range(block + 1):
-                expd = jnp.exp(pieces[pair] - peak)
-                total += jnp.sum(expd, axis=1, keepdims=True)
-                values = all_ref[2 * pair : 2 * pair + 2, :, 2 * value_width :].reshape(
-                    pair_rows, value_width
-                )
-                outcome += jnp.dot(
-                    expd.astype(jnp.bfloat16), values, preferred_element_type=jnp.float32
-                )
-            maps.append(outcome / total)
-        difference = maps[0] - head_weight * maps[1]
-        mean = jnp.mean(difference * difference, axis=1, keepdims=True)
-        heads[block] = (difference * lax.rsqrt(mean + norm_eps) * gain_ref[...]).astype(
-            jnp.bfloat16
-        )
-
-        @pl.when(z == block)
-        def _():
-            keeper(block).start()
-
-        @pl.when(z != block)
-        def _():
-            sender(block).start()
-
-    pass_on(0)
-    for block in range(n_z):
-        if len(pairs) <= block or 1 <= block + 1 < n_z - 1:
-            pass_on(len(pairs))
-        pairs[block].wait_recv()
-        attend(block)
+                copy.start()
+                scatter.append(copy)
+
+    @pl.when(odd == 1)
+    def _():
+        with jax.named_scope("odd0"):
+            for source in range(2):
+                wait_landed(below_kv.at[0, source], below_recv.at[source])
+            local_head(0, [below_piece])
+
+    @pl.when(z == 0)
+    def _():
+        with jax.named_scope("cross0"):
+            cross_head(1, 1, 1, [piece_of(own_kv, 1, 2, None)])
+
+    @pl.when(z == middle - 1)
+    def _():
+        with jax.named_scope("cross1"):
+            cross_head(0, middle, middle, [below_piece, piece_of(own_kv, 0, 2, None)])
+
+    @pl.when(z == middle)
+    def _():
+        with jax.named_scope("cross2"):
+            for source in range(2 * middle):
+                wait_landed(lower_kv.at[0, source], lower_recv.at[source])
+            local_head(1, [lower_piece])
+            cross_head(1, 1, middle + 1, [lower_piece, piece_of(own_kv, 1, 2, None)])
+
+    for j in range(share):
+
+        @pl.when(asks[j])
+        def _():
+            with jax.named_scope("finish"):
+                finish_upper(j)
+
+        @pl.when(jnp.logical_not(asks[j]))
+        def _():
+            for side in range(2):
+                low_diff[side * share + j] = jnp.zeros((row_count, head_width), jnp.bfloat16)
+
     total = partial[0].astype(jnp.float32)
-    for d in range(1, n_tp):
-        scatter[d - 1].wait_recv()
-        total += arrived[d].astype(jnp.float32)
+    with jax.named_scope("wait_part"):
+        for d in range(1, n_tp):
+            scatter[d - 1].wait_recv()
+            total += arrived[d].astype(jnp.float32)
     summed[...] = total.astype(jnp.bfloat16).reshape(n_ep, capacity, width)
     back = [pltpu.make_async_copy(summed.at[ep], returned.at[ep], local_sem.at[2])]
     for d in range(1, n_ep):
@@ -495,18 +725,34 @@
     for copy in back:
         copy.start()
 
-    for block in range(n_z):
-        keeper(block).wait()
+    with jax.named_scope("wait_heads"):
+        for j in range(share):
+            wait_landed(own_diff.at[other + j], diff_recv.at[other + j])
+
+        for j in range(share):
+
+            @pl.when(asks[j])
+            def _():
+                for side in range(2):
+                    at = side * share + j
+                    wait_landed(low_diff.at[at], cross_recv.at[at])
+
+    for head in range(head_count):
+        difference = own_diff[head].astype(jnp.float32) + low_diff[head].astype(jnp.float32)
+        mean = jnp.mean(difference * difference, axis=1, keepdims=True)
+        heads[head] = (difference * lax.rsqrt(mean + norm_eps) * gain_ref[...]).astype(
+            jnp.bfloat16
+        )
     weights[3].wait()
     mixed_scatter = []
     for d in list(range(1, n_tp)) + [0]:
         target = lax.rem(tp + d, n_tp)
         columns = pl.ds(pl.multiple_of(target * width, width), width)
         product = jnp.zeros((row_count, width), jnp.float32)
-        for h in range(n_z):
+        for h in range(head_count):
             product += jnp.dot(
-                landed[h],
-                weight_vmem[h * value_width : (h + 1) * value_width, columns],
+                heads[h],
+                weight_vmem[h * head_width : (h + 1) * head_width, columns],
                 preferred_element_type=jnp.float32,
             )
         mixed_partial[d] = product.astype(jnp.bfloat16)
@@ -516,9 +762,10 @@
             )
             copy.start()
             mixed_scatter.append(copy)
-    back[0].wait()
-    for copy in back[1:]:
-        copy.wait_recv()
+    with jax.named_scope("wait_back"):
+        back[0].wait()
+        for copy in back[1:]:
+            copy.wait_recv()
     flat = returned[...].reshape(rows, width)
     result = jnp.zeros(expert_ref.shape, jnp.float32)
     for k in range(picks):
@@ -532,19 +779,41 @@
         result += jnp.sum(spread_out, axis=1, keepdims=True) * picked
     expert_ref[...] = result.astype(expert_ref.dtype)
     total = mixed_partial[0].astype(jnp.float32)
-    for d in range(1, n_tp):
-        mixed_scatter[d - 1].wait_recv()
-        total += mixed_arrived[d].astype(jnp.float32)
+    with jax.named_scope("wait_mixed"):
+        for d in range(1, n_tp):
+            mixed_scatter[d - 1].wait_recv()
+            total += mixed_arrived[d].astype(jnp.float32)
     mixed_ref[...] = total.astype(jnp.bfloat16)
-    for copy in mixed_scatter:
+    for copy in dispatch[1:] + swaps + spread + scatter + back[1:] + mixed_scatter:
         copy.wait_send()
-    for block in range(n_z):
-
-        @pl.when(z != block)
-        def _():
-            sender(block).wait_send()
-    for copy in dispatch[1:] + exchange[1:] + spread + scatter + back[1:] + pairs:
-        copy.wait_send()
+    for j in range(share):
+        send_diff(j).wait_send()
+
+        @pl.when(asks[j])
+        def _():
+            send_stat(j).wait_send()
+            for side in range(2):
+                ask(side, j).wait_send()
+
+    for side in range(2):
+
+        @pl.when(odd == 0)
+        def _():
+            lift(side).wait_send()
+
+        @pl.when(z < middle)
+        def _():
+            lift_far(side).wait_send()
+
+        @pl.when(z <= middle)
+        def _():
+            send_cross(0, 0, side, z + 1).wait_send()
+            send_back(0, 0, side, z + 1).wait_send()
+
+        @pl.when(z == middle - 1)
+        def _():
+            send_cross(1, 0, side, z + 2).wait_send()
+            send_back(1, 0, side, z + 2).wait_send()
 
 
 def fused(
@@ -586,7 +855,8 @@
     vmem = pl.BlockSpec(memory_space=pltpu.VMEM)
     hbm = pl.BlockSpec(memory_space=pl.ANY)
     dma = pltpu.SemaphoreType.DMA
-    bf16 = jnp.bfloat16
+    bf16, f32 = jnp.bfloat16, jnp.float32
+    share = n_z // 2
     expert_out, mixed = pl.pallas_call(
         functools.partial(layer_kernel, n_ep, n_tp),
         out_shape=(
@@ -597,8 +867,22 @@
         out_specs=(vmem, vmem),
         scratch_shapes=[
             pltpu.VMEM((n_ep, capacity, width), bf16),
-            pltpu.VMEM((n_ep, row_count, 3 * head_width), bf16),
-            pltpu.VMEM((n_z, row_count, 3 * head_width), bf16),
+            pltpu.VMEM((n_z, row_count, head_width), bf16),
+            pltpu.VMEM((n_z, row_count, 2 * head_width), bf16),
+            pltpu.VMEM((share, 2, row_count, head_width), bf16),
+            pltpu.VMEM((share, 2, row_count, 2 * head_width), bf16),
+            pltpu.VMEM((1, 2, row_count, 2 * head_width), bf16),
+            pltpu.VMEM((1, n_z, row_count, 2 * head_width), bf16),
+            pltpu.VMEM((share, 2, row_count, head_width), bf16),
+            pltpu.VMEM((share, 2, 8, row_count), f32),
+            pltpu.VMEM((share, 2, 8, row_count), f32),
+            pltpu.VMEM((share, 2, 8, row_count), f32),
+            pltpu.VMEM((share, 2, 8, row_count), f32),
+            pltpu.VMEM((share, 2, 2, row_count, head_width), f32),
+            pltpu.VMEM((share, row_count, head_width), bf16),
+            pltpu.VMEM((n_z, row_count, head_width), bf16),
+            pltpu.VMEM((share, 2, row_count, head_width), bf16),
+            pltpu.VMEM((n_z, row_count, head_width), bf16),
             pltpu.VMEM((n_tp * n_ep, capacity, width), bf16),
             pltpu.VMEM(gate_weight.shape, bf16),
             pltpu.VMEM(up_weight.shape, bf16),
@@ -610,11 +894,10 @@
             pltpu.VMEM((n_ep, capacity, width), bf16),
             pltpu.VMEM(out_weight.shape, bf16),
             pltpu.VMEM((n_z, row_count, head_width), bf16),
-            pltpu.VMEM((n_z, row_count, head_width), bf16),
             pltpu.VMEM((n_tp, row_count, width), bf16),
             pltpu.VMEM((n_tp, row_count, width), bf16),
             dma((4,)),
-            dma((3,)),
+            dma((3 + n_z,)),
             dma((n_ep,)),
             dma((n_ep,)),
             dma((n_ep * n_tp,)),
@@ -623,11 +906,21 @@
             dma((n_tp,)),
             dma((n_ep,)),
             dma((n_ep,)),
+            dma((2, share)),
+            dma((2, share)),
+            dma((2,)),
+            dma((2,)),
+            dma((2,)),
             dma((n_z,)),
+            dma((2, share)),
+            dma((share, 2)),
+            dma((share,)),
+            dma((share,)),
+            dma((share, 2)),
+            dma((share, 2)),
+            dma((share,)),
             dma((n_z,)),
-            dma((n_z,)),
-            dma((n_z,)),
-            dma((n_z,)),
+            dma((share, 2)),
             dma((n_z,)),
             dma((n_tp,)),
             dma((n_tp,)),
@@ -676,6 +969,7 @@
     capacity = 3 * expert_rows.shape[0] * routes.shape[1] // (2 * n_ep)
     if (
         2 * head_count == n_ep
+        and head_count == 4
         and capacity % 16 == 0
         and value_rows.shape[1] == query_maps.shape[1] == 256 * head_count
     ):

time: 89.8 us -> 76.5 us (0.85)
  Pallas kernels: 84.3 us -> 71.1 us
    pallas_call x1, Pallas kernels: 84.3 us -> 71.1 us  [fused(): pl.pallas_call(functools.partial(layer_kernel, n_ep, n_tp), out_shape=(ja...]
where the time goes in v1:
time: 76.5 us; the launch traced here: 76.3 us
  Pallas kernels  71.1 us (93%)
  local copies, waits for them, and re-layouts  3.24 us (4%)
  other arithmetic  1.39 us (2%)
    pallas_call x1, Pallas kernels, fused(): pl.pallas_call(functools.partial(layer_kernel, n_ep, n_tp), out_shape=(ja...  71.1 us
    unnamed x2, local copies, waits for them, and re-layouts  3.24 us

profile of v1, /device:TPU:25, one launch (start us, length us, event | category | flops | bytes accessed | tf_op | source)
XLA Modules:
  0.0 76.3 jit_solution(3086749752603869371)
XLA Ops:
  0.7 0.5 fusion
  1.2 0.8 %pad_maximum_fusion = (f32[256,128]{1,0:T(8,128)}, f32[256,128]{1,0:T(8,128)}) fusion(f32[256,64]{1,0:T(8,128)S(1)} %get-tuple-element.8, f32[256,64]{1,0:T(8,128)S(1)} %get-tuple-element.7, f32[256,64]{1,0:T(8,128)S(1)} %get-tuple-element.6), kind=kLoop, calls=%fused_computation.2 | loop fusion | flops 65536 | bytes 458752 | tf_op jit(solution)/shard_map/concatenate | solution.py:852
  2.0 71.1 %layer.1 = (bf16[128,512]{1,0:T(8,128)(2,1)}, bf16[256,512]{1,0:T(8,128)(2,1)}) custom-call(bf16[128,2048]{1,0:T(8,128)(2,1)} %rows_ref.1, f32[1,2048]{1,0:T(1,128)} %bitcast.5, s32[2,128]{1,0:T(2,128)} %bitcast.6, f32[2,128]{1,0:T(2,128)} %bitcast.7, bf16[256,1024]{1,0:T(8,128)(2,1)} %query_ref.1, bf16[256,1024]{1,0:T(8,128)(2,1)} %key_ref.1, ...), custom_call_target="tpu_custom_call" | custom-call | tf_op jit(solution)/shard_map/layer/pallas_call | solution.py:860
  73.1 1.7 %copy.17 = bf16[256,512]{1,0:T(8,128)(2,1)} copy(bf16[256,512]{1,0:T(8,128)(2,1)} %get-tuple-element.13) | data formatting | bytes 524288
  74.8 1.6 %copy.18 = bf16[128,512]{1,0:T(8,128)(2,1)} copy(bf16[128,512]{1,0:T(8,128)(2,1)} %get-tuple-element.14) | data formatting | bytes 262144
  (2 shorter events, 0.0 us)

commit v2 on v1

--- a/solution.py
+++ b/solution.py
@@ -2,6 +2,7 @@
 
 import jax
 import jax.numpy as jnp
+import numpy as np
 from jax import lax
 from jax.experimental import pallas as pl
 from jax.experimental.pallas import tpu as pltpu
@@ -183,8 +184,8 @@
     query_ref,
     key_ref,
     value_ref,
-    cos_ref,
-    sin_ref,
+    turn_ref,
+    offset_ref,
     lambda_ref,
     gain_ref,
     gate_hbm,
@@ -251,6 +252,7 @@
     cross_recv,
     mixed_send,
     mixed_recv,
+    hold_sem,
 ):
     ep = lax.axis_index("ep")
     tp = lax.axis_index("tp")
@@ -317,14 +319,15 @@
     )
     with jax.named_scope("barrier"):
         pl.semaphore_wait(barrier, len(peers))
-    mine = tp * n_ep + ep
-    dispatch = [pltpu.make_async_copy(slots_ref.at[ep], gathered.at[mine], local_sem.at[0])]
+    across, along = tp + 1 - 2 * lax.rem(tp, 2), lax.rem(tp + 2, n_tp)
+    corner = n_tp - 1 - tp
+    dispatch = [pltpu.make_async_copy(slots_ref.at[ep], gathered.at[tp, 0], local_sem.at[0])]
     for d in range(1, n_ep):
         target = lax.rem(ep + d, n_ep)
         dispatch.append(
             remote(
                 slots_ref.at[target],
-                gathered.at[mine],
+                gathered.at[tp, d],
                 disp_send.at[d],
                 disp_recv.at[d],
                 {"ep": target},
@@ -333,13 +336,17 @@
     for copy in dispatch:
         copy.start()
 
+    cos_off, sin_off = offset_ref[0, pl.ds(ep, 1), :], offset_ref[1, pl.ds(ep, 1), :]
+    cosine = turn_ref[0] * cos_off - turn_ref[1] * sin_off
+    sine = turn_ref[1] * cos_off + turn_ref[0] * sin_off
+    sine = jnp.where(lax.broadcasted_iota(jnp.int32, sine.shape, 1) < half // 2, -sine, sine)
     for head in range(head_count):
         for m in range(2):
             at = head * head_width + m * half
             to = slice(m * half, (m + 1) * half)
             for ref, packed in ((query_ref, packed_q), (key_ref, packed_kv)):
                 entry = ref[:, at : at + half].astype(jnp.float32)
-                turned = entry * cos_ref[...] + pltpu.roll(entry, half // 2, 1) * sin_ref[...]
+                turned = entry * cosine + pltpu.roll(entry, half // 2, 1) * sine
                 packed[head, :, to] = turned.astype(jnp.bfloat16)
         packed_kv[head, :, head_width:] = value_ref[
             :, head * head_width : (head + 1) * head_width
@@ -407,19 +414,14 @@
     spread = []
     with jax.named_scope("wait_disp"):
         for d in range(n_ep):
-            source = lax.rem(ep + n_ep - d, n_ep)
             if d == 0:
                 dispatch[0].wait()
             else:
                 dispatch[d].wait_recv()
-            slot = gathered.at[tp * n_ep + source]
-            for t in range(1, n_tp):
+            slot = gathered.at[tp, d]
+            for way, device in enumerate((across, along)):
                 copy = remote(
-                    slot,
-                    slot,
-                    gath_send.at[d * n_tp + t],
-                    gath_recv.at[d * n_tp + t],
-                    {"tp": lax.rem(tp + t, n_tp)},
+                    slot, slot, gath_send.at[way, d], gath_recv.at[way, d], {"tp": device}
                 )
                 copy.start()
                 spread.append(copy)
@@ -524,11 +526,13 @@
             {"ep": 2 * host[j] + core},
         )
 
-    def local_head(j, pieces):
+    def wait_own(j):
         swaps[2 * j].wait_recv()
         swaps[2 * j + 1].wait_recv()
         keeps[2 * j].wait()
         keeps[2 * j + 1].wait()
+
+    def local_head(j, pieces):
         for block in range(2):
             mask = wide_causal if block else causal
             parts = pieces + [piece_of(own_kv, j, block + 1, mask)]
@@ -616,62 +620,87 @@
     @pl.when(z != middle)
     def _():
         with jax.named_scope("own1"):
+            wait_own(1)
             local_head(1, [])
 
     @pl.when(odd == 0)
     def _():
         with jax.named_scope("own0"):
+            wait_own(0)
             local_head(0, [])
 
-    with jax.named_scope("wait_gath"):
-        for copy in spread:
-            copy.wait_recv()
-    weights[0].wait()
-    weights[1].wait()
+    with jax.named_scope("forward"):
+        for d in range(n_ep):
+            way = d % 2
+            slot = gathered.at[(across, along)[way], d]
+            wait_landed(slot, gath_recv.at[way, d])
+            copy = remote(
+                slot, slot, gath_send.at[2, d], gath_recv.at[2, d], {"tp": (along, across)[way]}
+            )
+            copy.start()
+            spread.append(copy)
     tile = 256
-
-    def hidden_tile(j, carry):
-        columns = pl.ds(pl.multiple_of(j * tile, tile), tile)
-        gate = jnp.zeros((rows, tile), jnp.float32)
-        up = jnp.zeros((rows, tile), jnp.float32)
-        for i in range(n_tp):
-            block = gathered[i * n_ep : (i + 1) * n_ep].reshape(rows, width)
-            gate += jnp.dot(
-                block,
-                gate_vmem[0, i * width : (i + 1) * width, columns],
-                preferred_element_type=jnp.float32,
-            )
-            up += jnp.dot(
-                block,
-                up_vmem[0, i * width : (i + 1) * width, columns],
-                preferred_element_type=jnp.float32,
-            )
-        hidden[:, columns] = (gate / (1.0 + jnp.exp(-gate)) * up).astype(jnp.bfloat16)
-        return carry
-
-    with jax.named_scope("gateup"):
-        lax.fori_loop(0, hidden.shape[1] // tile, hidden_tile, 0)
-    weights[2].wait()
+    part_count = n_ep // 2
+    part_rows = part_count * capacity
     scatter = []
-    with jax.named_scope("down"):
-        for d in list(range(1, n_tp)) + [0]:
-            target = lax.rem(tp + d, n_tp)
-            columns = pl.ds(pl.multiple_of(target * width, width), width)
-            partial[d] = jnp.dot(
-                hidden[...], down_vmem[0, :, columns], preferred_element_type=jnp.float32
-            ).astype(jnp.bfloat16)
-            if d:
-                copy = remote(
-                    partial.at[d], arrived.at[d], part_send.at[d], part_recv.at[d], {"tp": target}
+    for part in range(2):
+        lead = part * part_count
+        with jax.named_scope(f"wait_gath#p={part}"):
+            for d in range(lead, lead + part_count):
+                way = 1 - d % 2
+                wait_landed(gathered.at[(across, along)[way], d], gath_recv.at[way, d])
+                wait_landed(gathered.at[corner, d], gath_recv.at[2, d])
+        if part == 0:
+            weights[0].wait()
+            weights[1].wait()
+
+        def hidden_tile(j, carry):
+            columns = pl.ds(pl.multiple_of(j * tile, tile), tile)
+            gate = jnp.zeros((part_rows, tile), jnp.float32)
+            up = jnp.zeros((part_rows, tile), jnp.float32)
+            for i in range(n_tp):
+                block = gathered[i, lead : lead + part_count].reshape(part_rows, width)
+                gate += jnp.dot(
+                    block,
+                    gate_vmem[0, i * width : (i + 1) * width, columns],
+                    preferred_element_type=jnp.float32,
                 )
-                copy.start()
-                scatter.append(copy)
+                up += jnp.dot(
+                    block,
+                    up_vmem[0, i * width : (i + 1) * width, columns],
+                    preferred_element_type=jnp.float32,
+                )
+            hidden[part, :, columns] = (gate / (1.0 + jnp.exp(-gate)) * up).astype(jnp.bfloat16)
+            return carry
+
+        with jax.named_scope(f"gateup#p={part}"):
+            lax.fori_loop(0, hidden.shape[2] // tile, hidden_tile, 0)
+        if part == 0:
+            weights[2].wait()
+        with jax.named_scope(f"down#p={part}"):
+            for d in list(range(1, n_tp)) + [0]:
+                target = lax.rem(tp + d, n_tp)
+                columns = pl.ds(pl.multiple_of(target * width, width), width)
+                partial[part, d] = jnp.dot(
+                    hidden[part], down_vmem[0, :, columns], preferred_element_type=jnp.float32
+                ).astype(jnp.bfloat16)
+                if d:
+                    copy = remote(
+                        partial.at[part, d],
+                        arrived.at[part, d],
+                        part_send.at[part, d],
+                        part_recv.at[part, d],
+                        {"tp": target},
+                    )
+                    copy.start()
+                    scatter.append(copy)
 
     @pl.when(odd == 1)
     def _():
         with jax.named_scope("odd0"):
             for source in range(2):
                 wait_landed(below_kv.at[0, source], below_recv.at[source])
+            wait_own(0)
             local_head(0, [below_piece])
 
     @pl.when(z == 0)
@@ -683,85 +712,157 @@
     def _():
         with jax.named_scope("cross1"):
             cross_head(0, middle, middle, [below_piece, piece_of(own_kv, 0, 2, None)])
+
+    def project():
+        with jax.named_scope("wait_heads"):
+            for j in range(share):
+                wait_landed(own_diff.at[other + j], diff_recv.at[other + j])
+
+                @pl.when(asks[j])
+                def _():
+                    for side in range(2):
+                        at = side * share + j
+                        wait_landed(low_diff.at[at], cross_recv.at[at])
+
+        for head in range(head_count):
+            difference = own_diff[head].astype(jnp.float32) + low_diff[head].astype(jnp.float32)
+            mean = jnp.mean(difference * difference, axis=1, keepdims=True)
+            heads[head] = (difference * lax.rsqrt(mean + norm_eps) * gain_ref[...]).astype(
+                jnp.bfloat16
+            )
+        weights[3].wait()
+        for d in list(range(1, n_tp)) + [0]:
+            target = lax.rem(tp + d, n_tp)
+            columns = pl.ds(pl.multiple_of(target * width, width), width)
+            product = jnp.zeros((row_count, width), jnp.float32)
+            for h in range(head_count):
+                product += jnp.dot(
+                    heads[h],
+                    weight_vmem[h * head_width : (h + 1) * head_width, columns],
+                    preferred_element_type=jnp.float32,
+                )
+            mixed_partial[d] = product.astype(jnp.bfloat16)
+            if d:
+                mixed_copy(d).start()
+
+    def mixed_copy(d):
+        return remote(
+            mixed_partial.at[d],
+            mixed_arrived.at[d],
+            mixed_send.at[d],
+            mixed_recv.at[d],
+            {"tp": lax.rem(tp + d, n_tp)},
+        )
+
+    back = []
+    for d in range(n_ep):
+        if d == 0:
+            copy = pltpu.make_async_copy(summed.at[0], returned.at[ep], local_sem.at[2])
+        else:
+            copy = remote(
+                summed.at[d],
+                returned.at[ep],
+                ret_send.at[d],
+                ret_recv.at[d],
+                {"ep": lax.rem(ep + n_ep - d, n_ep)},
+            )
+        back.append(copy)
+
+    def sum_part(part):
+        lead = part * part_count
+        total = partial[part, 0].astype(jnp.float32)
+        with jax.named_scope(f"wait_part#p={part}"):
+            for d in range(1, n_tp):
+                scatter[part * (n_tp - 1) + d - 1].wait_recv()
+                total += arrived[part, d].astype(jnp.float32)
+        summed[lead : lead + part_count] = total.astype(jnp.bfloat16).reshape(
+            part_count, capacity, width
+        )
+
+    for j in range(share):
+
+        @pl.when(jnp.logical_not(asks[j]))
+        def _():
+            for side in range(2):
+                low_diff[side * share + j] = jnp.zeros((row_count, head_width), jnp.bfloat16)
+
+    @pl.when(z == middle - 1)
+    def _():
+        with jax.named_scope("finish"):
+            finish_upper(1)
+
+    @pl.when(z < middle)
+    def _():
+        with jax.named_scope("project_low"):
+            project()
+
+    sum_part(0)
+
+    @pl.when(z >= middle)
+    def _():
+        for copy in back[:part_count]:
+            copy.start()
 
     @pl.when(z == middle)
     def _():
         with jax.named_scope("cross2"):
             for source in range(2 * middle):
                 wait_landed(lower_kv.at[0, source], lower_recv.at[source])
+            wait_own(1)
+            cross_head(1, 1, middle + 1, [lower_piece, piece_of(own_kv, 1, 2, None)])
             local_head(1, [lower_piece])
-            cross_head(1, 1, middle + 1, [lower_piece, piece_of(own_kv, 1, 2, None)])
-
-    for j in range(share):
-
-        @pl.when(asks[j])
+
+    sum_part(1)
+
+    @pl.when(z < middle)
+    def _():
+        targets = [lax.rem(ep + n_ep - d, n_ep) for d in range(n_ep)]
+        for target, copy in zip(targets, back):
+
+            @pl.when(target < 2 * middle)
+            def _():
+                copy.start()
+
+        with jax.named_scope("hold"):
+
+            @pl.when(z == middle - 1)
+            def _():
+                for up in range(middle):
+                    for side in range(2):
+                        send_cross(up, 0, side, middle + up).wait_send()
+                pl.semaphore_signal(
+                    hold_sem,
+                    inc=1,
+                    device_id={"ep": lax.rem(ep + n_ep - 2, n_ep)},
+                    device_id_type=MESH,
+                )
+
+            @pl.when(z != middle - 1)
+            def _():
+                pl.semaphore_wait(hold_sem, 1)
+
+        for target, copy in zip(targets, back):
+
+            @pl.when(target >= 2 * middle)
+            def _():
+                copy.start()
+
+    @pl.when(z >= middle)
+    def _():
+        for copy in back[part_count:]:
+            copy.start()
+
+        with jax.named_scope("finish"):
+            finish_upper(0)
+
+        @pl.when(odd == 1)
         def _():
             with jax.named_scope("finish"):
-                finish_upper(j)
-
-        @pl.when(jnp.logical_not(asks[j]))
-        def _():
-            for side in range(2):
-                low_diff[side * share + j] = jnp.zeros((row_count, head_width), jnp.bfloat16)
-
-    total = partial[0].astype(jnp.float32)
-    with jax.named_scope("wait_part"):
-        for d in range(1, n_tp):
-            scatter[d - 1].wait_recv()
-            total += arrived[d].astype(jnp.float32)
-    summed[...] = total.astype(jnp.bfloat16).reshape(n_ep, capacity, width)
-    back = [pltpu.make_async_copy(summed.at[ep], returned.at[ep], local_sem.at[2])]
-    for d in range(1, n_ep):
-        target = lax.rem(ep + d, n_ep)
-        back.append(
-            remote(
-                summed.at[target],
-                returned.at[ep],
-                ret_send.at[d],
-                ret_recv.at[d],
-                {"ep": target},
-            )
-        )
-    for copy in back:
-        copy.start()
-
-    with jax.named_scope("wait_heads"):
-        for j in range(share):
-            wait_landed(own_diff.at[other + j], diff_recv.at[other + j])
-
-        for j in range(share):
-
-            @pl.when(asks[j])
-            def _():
-                for side in range(2):
-                    at = side * share + j
-                    wait_landed(low_diff.at[at], cross_recv.at[at])
-
-    for head in range(head_count):
-        difference = own_diff[head].astype(jnp.float32) + low_diff[head].astype(jnp.float32)
-        mean = jnp.mean(difference * difference, axis=1, keepdims=True)
-        heads[head] = (difference * lax.rsqrt(mean + norm_eps) * gain_ref[...]).astype(
-            jnp.bfloat16
-        )
-    weights[3].wait()
-    mixed_scatter = []
-    for d in list(range(1, n_tp)) + [0]:
-        target = lax.rem(tp + d, n_tp)
-        columns = pl.ds(pl.multiple_of(target * width, width), width)
-        product = jnp.zeros((row_count, width), jnp.float32)
-        for h in range(head_count):
-            product += jnp.dot(
-                heads[h],
-                weight_vmem[h * head_width : (h + 1) * head_width, columns],
-                preferred_element_type=jnp.float32,
-            )
-        mixed_partial[d] = product.astype(jnp.bfloat16)
-        if d:
-            copy = remote(
-                mixed_partial.at[d], mixed_arrived.at[d], mixed_send.at[d], mixed_recv.at[d], {"tp": target}
-            )
-            copy.start()
-            mixed_scatter.append(copy)
+                finish_upper(1)
+
+        with jax.named_scope("project_up"):
+            project()
+
     with jax.named_scope("wait_back"):
         back[0].wait()
         for copy in back[1:]:
@@ -781,11 +882,13 @@
     total = mixed_partial[0].astype(jnp.float32)
     with jax.named_scope("wait_mixed"):
         for d in range(1, n_tp):
-            mixed_scatter[d - 1].wait_recv()
+            mixed_copy(d).wait_recv()
             total += mixed_arrived[d].astype(jnp.float32)
     mixed_ref[...] = total.astype(jnp.bfloat16)
-    for copy in dispatch[1:] + swaps + spread + scatter + back[1:] + mixed_scatter:
+    for copy in dispatch[1:] + swaps + spread + scatter + back[1:]:
         copy.wait_send()
+    for d in range(1, n_tp):
+        mixed_copy(d).wait_send()
     for j in range(share):
         send_diff(j).wait_send()
 
@@ -807,13 +910,20 @@
 
         @pl.when(z <= middle)
         def _():
-            send_cross(0, 0, side, z + 1).wait_send()
             send_back(0, 0, side, z + 1).wait_send()
+
+            @pl.when(z != middle - 1)
+            def _():
+                send_cross(0, 0, side, z + 1).wait_send()
 
         @pl.when(z == middle - 1)
         def _():
-            send_cross(1, 0, side, z + 2).wait_send()
             send_back(1, 0, side, z + 2).wait_send()
+
+
+def hand_over(expert_ref, mixed_ref, expert_out, mixed_out):
+    expert_out[...] = expert_ref[...]
+    mixed_out[...] = mixed_ref[...]
 
 
 def fused(
@@ -834,7 +944,6 @@
     n_ep = lax.axis_size("ep")
     n_tp = lax.axis_size("tp")
     n_z = n_ep // 2
-    ep = lax.axis_index("ep")
     row_count = query_maps.shape[0]
     head_width = query_maps.shape[1] // n_z
     head_dim = head_width // 2
@@ -844,13 +953,13 @@
     hidden_width = gate_weight.shape[2]
     slot_rows = n_ep * capacity
 
-    positions = ep * row_count + jnp.arange(row_count, dtype=jnp.int32)
     half_dim = head_dim // 2
-    inverse = rope_base ** (-2.0 * jnp.arange(half_dim, dtype=jnp.float32) / head_dim)
-    angles = positions.astype(jnp.float32)[:, None] * inverse[None, :]
-    cosine, sine = jnp.cos(angles), jnp.sin(angles)
-    cos_table = jnp.concatenate([cosine, cosine], axis=1)
-    sin_table = jnp.concatenate([-sine, sine], axis=1)
+    inverse = rope_base ** (-2.0 * np.arange(half_dim) / head_dim)
+    inverse = np.concatenate([inverse, inverse])
+    turns = np.arange(row_count)[:, None] * inverse
+    offsets = (row_count * np.arange(n_ep))[:, None] * inverse
+    turns = jnp.asarray(np.stack([np.cos(turns), np.sin(turns)]), jnp.float32)
+    offsets = jnp.asarray(np.stack([np.cos(offsets), np.sin(offsets)]), jnp.float32)
 
     vmem = pl.BlockSpec(memory_space=pltpu.VMEM)
     hbm = pl.BlockSpec(memory_space=pl.ANY)
@@ -883,13 +992,13 @@
             pltpu.VMEM((n_z, row_count, head_width), bf16),
             pltpu.VMEM((share, 2, row_count, head_width), bf16),
             pltpu.VMEM((n_z, row_count, head_width), bf16),
-            pltpu.VMEM((n_tp * n_ep, capacity, width), bf16),
+            pltpu.VMEM((n_tp, n_ep, capacity, width), bf16),
             pltpu.VMEM(gate_weight.shape, bf16),
             pltpu.VMEM(up_weight.shape, bf16),
             pltpu.VMEM(down_weight.shape, bf16),
-            pltpu.VMEM((slot_rows, hidden_width), bf16),
-            pltpu.VMEM((n_tp, slot_rows, width), bf16),
-            pltpu.VMEM((n_tp, slot_rows, width), bf16),
+            pltpu.VMEM((2, slot_rows // 2, hidden_width), bf16),
+            pltpu.VMEM((2, n_tp, slot_rows // 2, width), bf16),
+            pltpu.VMEM((2, n_tp, slot_rows // 2, width), bf16),
             pltpu.VMEM((n_ep, capacity, width), bf16),
             pltpu.VMEM((n_ep, capacity, width), bf16),
             pltpu.VMEM(out_weight.shape, bf16),
@@ -900,10 +1009,10 @@
             dma((3 + n_z,)),
             dma((n_ep,)),
             dma((n_ep,)),
-            dma((n_ep * n_tp,)),
-            dma((n_ep * n_tp,)),
-            dma((n_tp,)),
-            dma((n_tp,)),
+            dma((3, n_ep)),
+            dma((3, n_ep)),
+            dma((2, n_tp)),
+            dma((2, n_tp)),
             dma((n_ep,)),
             dma((n_ep,)),
             dma((2, share)),
@@ -924,6 +1033,7 @@
             dma((n_z,)),
             dma((n_tp,)),
             dma((n_tp,)),
+            pltpu.SemaphoreType.REGULAR,
         ],
         compiler_params=pltpu.CompilerParams(
             collective_id=0, has_side_effects=True, vmem_limit_bytes=60 * 1024 * 1024
@@ -937,8 +1047,8 @@
         query_maps,
         key_maps,
         value_rows,
-        cos_table,
-        sin_table,
+        turns,
+        offsets,
         head_lambda.reshape(1, n_z),
         head_gain.reshape(1, head_width),
         gate_weight,
@@ -946,6 +1056,16 @@
         down_weight,
         out_weight,
     )
+    expert_out, mixed = pl.pallas_call(
+        hand_over,
+        out_shape=(
+            jax.ShapeDtypeStruct((token_count, width), bf16),
+            jax.ShapeDtypeStruct((row_count, width), bf16),
+        ),
+        in_specs=[vmem] * 2,
+        out_specs=(vmem, vmem),
+        name="hand_over",
+    )(expert_out, mixed)
     return (mixed, expert_out)
 
 
@@ -969,7 +1089,7 @@
     capacity = 3 * expert_rows.shape[0] * routes.shape[1] // (2 * n_ep)
     if (
         2 * head_count == n_ep
-        and head_count == 4
+        and head_count == lax.axis_size("tp") == 4
         and capacity % 16 == 0
         and value_rows.shape[1] == query_maps.shape[1] == 256 * head_count
     ):

time: 76.5 us -> 69.5 us (0.908)
  local copies, waits for them, and re-layouts: 3.24 us -> 0 us
  Pallas kernels: 71.1 us -> 68.6 us
  other arithmetic: 1.39 us -> 0 us
    pallas_call x1, Pallas kernels: 71.1 us -> 66.9 us  [fused(): pl.pallas_call(functools.partial(layer_kernel, n_ep, n_tp), out_shape=(ja...]
    unnamed x2 -> x0, local copies, waits for them, and re-layouts: 3.24 us -> none
    pallas_call x0 -> x1, Pallas kernels: none -> 1.78 us  [fused(): pl.pallas_call(hand_over, out_shape=(jax.ShapeDtypeStruct((token_count, w...]
    concatenate x1 -> x0, other arithmetic: 0.84 us -> none  [fused(): cos_table = jnp.concatenate([cosine, cosine], axis=1)]
where the time goes in v2:
time: 69.5 us; the launch traced here: 69.3 us
  Pallas kernels  68.6 us (99%)
    pallas_call x1, Pallas kernels, fused(): pl.pallas_call(functools.partial(layer_kernel, n_ep, n_tp), out_shape=(ja...  66.9 us
    pallas_call x1, Pallas kernels, fused(): pl.pallas_call(hand_over, out_shape=(jax.ShapeDtypeStruct((token_count, w...  1.78 us

profile of v2, /device:TPU:25, one launch (start us, length us, event | category | flops | bytes accessed | tf_op | source)
XLA Modules:
  0.0 69.3 jit_solution(15698634605926437011)
XLA Ops:
  0.6 66.9 %layer.1 = (bf16[128,512]{1,0:T(8,128)(2,1)}, bf16[256,512]{1,0:T(8,128)(2,1)}) custom-call(bf16[128,2048]{1,0:T(8,128)(2,1)} %rows_ref.1, f32[1,2048]{1,0:T(1,128)} %bitcast.5, s32[2,128]{1,0:T(2,128)} %bitcast.6, f32[2,128]{1,0:T(2,128)} %bitcast.7, bf16[256,1024]{1,0:T(8,128)(2,1)} %query_ref.1, bf16[256,1024]{1,0:T(8,128)(2,1)} %key_ref.1, ...), custom_call_target="tpu_custom_call" | custom-call | tf_op jit(solution)/shard_map/layer/pallas_call | solution.py:969
  67.5 1.8 %hand_over.1 = (bf16[128,512]{1,0:T(8,128)(2,1)}, bf16[256,512]{1,0:T(8,128)(2,1)}) custom-call(bf16[128,512]{1,0:T(8,128)(2,1)} %get-tuple-element.6.expert_ref, bf16[256,512]{1,0:T(8,128)(2,1)} %get-tuple-element.7.mixed_ref), custom_call_target="tpu_custom_call" | custom-call | tf_op jit(solution)/shard_map/hand_over/pallas_call | solution.py:1059

commit v3 on v2

--- a/solution.py
+++ b/solution.py
@@ -224,6 +224,7 @@
     heads,
     mixed_partial,
     mixed_arrived,
+    mixed_sum,
     weight_sem,
     local_sem,
     disp_send,
@@ -731,8 +732,7 @@
                 jnp.bfloat16
             )
         weights[3].wait()
-        for d in list(range(1, n_tp)) + [0]:
-            target = lax.rem(tp + d, n_tp)
+        for role, target in ((3, corner), (1, across), (2, along), (0, tp)):
             columns = pl.ds(pl.multiple_of(target * width, width), width)
             product = jnp.zeros((row_count, width), jnp.float32)
             for h in range(head_count):
@@ -741,18 +741,34 @@
                     weight_vmem[h * head_width : (h + 1) * head_width, columns],
                     preferred_element_type=jnp.float32,
                 )
-            mixed_partial[d] = product.astype(jnp.bfloat16)
-            if d:
-                mixed_copy(d).start()
-
-    def mixed_copy(d):
+            mixed_partial[role] = product.astype(jnp.bfloat16).reshape(
+                2, row_count // 2, width
+            )
+            for part in range(2):
+                if role == 3:
+                    mixed_copy(1, part).start()
+                elif role == 1 + part:
+                    mixed_copy(0, part).start()
+
+    ways = (across, along)
+
+    def mixed_copy(kind, part):
         return remote(
-            mixed_partial.at[d],
-            mixed_arrived.at[d],
-            mixed_send.at[d],
-            mixed_recv.at[d],
-            {"tp": lax.rem(tp + d, n_tp)},
-        )
+            (mixed_partial.at[1 + part, part], mixed_partial.at[3, part], mixed_sum.at[part])[kind],
+            mixed_arrived.at[kind, part],
+            mixed_send.at[kind, part],
+            mixed_recv.at[kind, part],
+            {"tp": ways[1 - part if kind == 2 else part]},
+        )
+
+    def mixed_forward():
+        with jax.named_scope("mixed_forward"):
+            for part in range(2):
+                mixed_copy(1, part).wait_recv()
+                both = mixed_partial[2 - part, part].astype(jnp.float32)
+                both += mixed_arrived[1, part].astype(jnp.float32)
+                mixed_sum[part] = both.astype(jnp.bfloat16)
+                mixed_copy(2, part).start()
 
     back = []
     for d in range(n_ep):
@@ -798,6 +814,10 @@
 
     sum_part(0)
 
+    @pl.when(z < middle)
+    def _():
+        mixed_forward()
+
     @pl.when(z >= middle)
     def _():
         for copy in back[:part_count]:
@@ -814,6 +834,14 @@
 
     sum_part(1)
 
+    def release():
+        pl.semaphore_signal(
+            hold_sem,
+            inc=1,
+            device_id={"ep": lax.rem(ep + n_ep - 2, n_ep)},
+            device_id_type=MESH,
+        )
+
     @pl.when(z < middle)
     def _():
         targets = [lax.rem(ep + n_ep - d, n_ep) for d in range(n_ep)]
@@ -830,12 +858,8 @@
                 for up in range(middle):
                     for side in range(2):
                         send_cross(up, 0, side, middle + up).wait_send()
-                pl.semaphore_signal(
-                    hold_sem,
-                    inc=1,
-                    device_id={"ep": lax.rem(ep + n_ep - 2, n_ep)},
-                    device_id_type=MESH,
-                )
+                pl.semaphore_wait(hold_sem, 1)
+                release()
 
             @pl.when(z != middle - 1)
             def _():
@@ -849,8 +873,10 @@
 
     @pl.when(z >= middle)
     def _():
-        for copy in back[part_count:]:
-            copy.start()
+        @pl.when(z != middle)
+        def _():
+            for copy in back[part_count:]:
+                copy.start()
 
         with jax.named_scope("finish"):
             finish_upper(0)
@@ -862,6 +888,17 @@
 
         with jax.named_scope("project_up"):
             project()
+
+        @pl.when(z == middle)
+        def _():
+            with jax.named_scope("held"):
+                for side in range(2):
+                    send_cross(0, 1, side, middle + 1).wait_send()
+            release()
+            for copy in back[part_count:]:
+                copy.start()
+
+        mixed_forward()
 
     with jax.named_scope("wait_back"):
         back[0].wait()
@@ -879,16 +916,19 @@
         spread_out = jnp.where(before == after, route_weights_ref[k : k + 1, :], 0.0)
         result += jnp.sum(spread_out, axis=1, keepdims=True) * picked
     expert_ref[...] = result.astype(expert_ref.dtype)
-    total = mixed_partial[0].astype(jnp.float32)
     with jax.named_scope("wait_mixed"):
-        for d in range(1, n_tp):
-            mixed_copy(d).wait_recv()
-            total += mixed_arrived[d].astype(jnp.float32)
-    mixed_ref[...] = total.astype(jnp.bfloat16)
+        for part in range(2):
+            total = mixed_partial[0, part].astype(jnp.float32)
+            for kind in (0, 2):
+                mixed_copy(kind, part).wait_recv()
+                total += mixed_arrived[kind, part].astype(jnp.float32)
+            lines = slice(part * row_count // 2, (part + 1) * row_count // 2)
+            mixed_ref[lines, :] = total.astype(jnp.bfloat16)
     for copy in dispatch[1:] + swaps + spread + scatter + back[1:]:
         copy.wait_send()
-    for d in range(1, n_tp):
-        mixed_copy(d).wait_send()
+    for kind in range(3):
+        for part in range(2):
+            mixed_copy(kind, part).wait_send()
     for j in range(share):
         send_diff(j).wait_send()
 
@@ -912,7 +952,7 @@
         def _():
             send_back(0, 0, side, z + 1).wait_send()
 
-            @pl.when(z != middle - 1)
+            @pl.when(z < middle - 1)
             def _():
                 send_cross(0, 0, side, z + 1).wait_send()
 
@@ -1003,8 +1043,9 @@
             pltpu.VMEM((n_ep, capacity, width), bf16),
             pltpu.VMEM(out_weight.shape, bf16),
             pltpu.VMEM((n_z, row_count, head_width), bf16),
-            pltpu.VMEM((n_tp, row_count, width), bf16),
-            pltpu.VMEM((n_tp, row_count, width), bf16),
+            pltpu.VMEM((n_tp, 2, row_count // 2, width), bf16),
+            pltpu.VMEM((3, 2, row_count // 2, width), bf16),
+            pltpu.VMEM((2, row_count // 2, width), bf16),
             dma((4,)),
             dma((3 + n_z,)),
             dma((n_ep,)),
@@ -1031,8 +1072,8 @@
             dma((n_z,)),
             dma((share, 2)),
             dma((n_z,)),
-            dma((n_tp,)),
-            dma((n_tp,)),
+            dma((3, 2)),
+            dma((3, 2)),
             pltpu.SemaphoreType.REGULAR,
         ],
         compiler_params=pltpu.CompilerParams(

time: 69.5 us -> 66.7 us (0.960)
  Pallas kernels: 68.6 us -> 65.2 us
    pallas_call x1, Pallas kernels: 66.9 us -> 63.4 us  [fused(): pl.pallas_call(functools.partial(layer_kernel, n_ep, n_tp), out_shape=(ja...]
where the time goes in v3:
time: 66.7 us; the launch traced here: 65.8 us
  Pallas kernels  65.2 us (98%)
    pallas_call x1, Pallas kernels, fused(): pl.pallas_call(functools.partial(layer_kernel, n_ep, n_tp), out_shape=(ja...  63.4 us
    pallas_call x1, Pallas kernels, fused(): pl.pallas_call(hand_over, out_shape=(jax.ShapeDtypeStruct((token_count, w...  1.78 us

profile of v3, /device:TPU:25, one launch (start us, length us, event | category | flops | bytes accessed | tf_op | source)
XLA Modules:
  0.0 65.8 jit_solution(5946436465819651294)
XLA Ops:
  0.6 63.4 %layer.1 = (bf16[128,512]{1,0:T(8,128)(2,1)}, bf16[256,512]{1,0:T(8,128)(2,1)}) custom-call(bf16[128,2048]{1,0:T(8,128)(2,1)} %rows_ref.1, f32[1,2048]{1,0:T(1,128)} %bitcast.5, s32[2,128]{1,0:T(2,128)} %bitcast.6, f32[2,128]{1,0:T(2,128)} %bitcast.7, bf16[256,1024]{1,0:T(8,128)(2,1)} %query_ref.1, bf16[256,1024]{1,0:T(8,128)(2,1)} %key_ref.1, ...), custom_call_target="tpu_custom_call" | custom-call | tf_op jit(solution)/shard_map/layer/pallas_call | solution.py:1009
  64.1 1.8 %hand_over.1 = (bf16[128,512]{1,0:T(8,128)(2,1)}, bf16[256,512]{1,0:T(8,128)(2,1)}) custom-call(bf16[128,512]{1,0:T(8,128)(2,1)} %get-tuple-element.6.expert_ref, bf16[256,512]{1,0:T(8,128)(2,1)} %get-tuple-element.7.mixed_ref), custom_call_target="tpu_custom_call" | custom-call | tf_op jit(solution)/shard_map/hand_over/pallas_call | solution.py:1100

commit v4 on v3

--- a/solution.py
+++ b/solution.py
@@ -177,23 +177,28 @@
 def layer_kernel(
     n_ep,
     n_tp,
-    rows_ref,
     norm_gain_ref,
     routes_ref,
     route_weights_ref,
-    query_ref,
-    key_ref,
-    value_ref,
-    turn_ref,
     offset_ref,
     lambda_ref,
     gain_ref,
+    rows_hbm,
+    query_hbm,
+    key_hbm,
+    value_hbm,
+    turn_hbm,
     gate_hbm,
     up_hbm,
     down_hbm,
     weight_hbm,
     expert_ref,
     mixed_ref,
+    rows_ref,
+    query_ref,
+    key_ref,
+    value_ref,
+    turn_ref,
     slots_ref,
     packed_q,
     packed_kv,
@@ -225,6 +230,7 @@
     mixed_partial,
     mixed_arrived,
     mixed_sum,
+    input_sem,
     weight_sem,
     local_sem,
     disp_send,
@@ -277,7 +283,14 @@
         pltpu.make_async_copy(down_hbm, down_vmem, weight_sem.at[2]),
         pltpu.make_async_copy(weight_hbm, weight_vmem, weight_sem.at[3]),
     ]
-    for copy in weights:
+    inputs = [
+        pltpu.make_async_copy(rows_hbm, rows_ref, input_sem.at[0]),
+        pltpu.make_async_copy(turn_hbm, turn_ref, input_sem.at[1]),
+        pltpu.make_async_copy(query_hbm, query_ref, input_sem.at[2]),
+        pltpu.make_async_copy(key_hbm, key_ref, input_sem.at[3]),
+        pltpu.make_async_copy(value_hbm, value_ref, input_sem.at[4]),
+    ]
+    for copy in inputs:
         copy.start()
     peers = [{"ep": lax.rem(ep + d, n_ep)} for d in range(1, n_ep)]
     peers += [{"tp": lax.rem(tp + d, n_tp)} for d in range(1, n_tp)]
@@ -287,6 +300,9 @@
 
     token_count = rows_ref.shape[0]
     picks = routes_ref.shape[0]
+    inputs[0].wait()
+    for copy in weights:
+        copy.start()
     entries = rows_ref[...].astype(jnp.float32)
     inverse_norm = lax.rsqrt(jnp.mean(entries * entries, axis=1, keepdims=True) + norm_eps)
     own = pl.ds(pl.multiple_of(tp * width, width), width)
@@ -337,6 +353,8 @@
     for copy in dispatch:
         copy.start()
 
+    for copy in inputs[1:]:
+        copy.wait()
     cos_off, sin_off = offset_ref[0, pl.ds(ep, 1), :], offset_ref[1, pl.ds(ep, 1), :]
     cosine = turn_ref[0] * cos_off - turn_ref[1] * sin_off
     sine = turn_ref[1] * cos_off + turn_ref[0] * sin_off
@@ -412,9 +430,31 @@
     def wait_landed(ref, sem):
         pltpu.make_async_copy(ref, ref, sem).wait()
 
+    def leave():
+        for j in range(share):
+            for side in range(2):
+
+                @pl.when(asks[j])
+                def _():
+                    ask(side, j).start()
+
+        for side in range(2):
+
+            @pl.when(odd == 0)
+            def _():
+                lift(side).start()
+
+        for side in range(2):
+
+            @pl.when(z < middle)
+            def _():
+                lift_far(side).start()
+
     spread = []
     with jax.named_scope("wait_disp"):
         for d in range(n_ep):
+            if d == 5:
+                leave()
             if d == 0:
                 dispatch[0].wait()
             else:
@@ -426,25 +466,6 @@
                 )
                 copy.start()
                 spread.append(copy)
-
-    for j in range(share):
-        for side in range(2):
-
-            @pl.when(asks[j])
-            def _():
-                ask(side, j).start()
-
-    for side in range(2):
-
-        @pl.when(odd == 0)
-        def _():
-            lift(side).start()
-
-    for side in range(2):
-
-        @pl.when(z < middle)
-        def _():
-            lift_far(side).start()
 
     row = lax.broadcasted_iota(jnp.int32, (row_count, row_count), 0)
     column = lax.broadcasted_iota(jnp.int32, (row_count, row_count), 1)
@@ -1012,9 +1033,14 @@
             jax.ShapeDtypeStruct((token_count, width), bf16),
             jax.ShapeDtypeStruct((row_count, width), bf16),
         ),
-        in_specs=[vmem] * 11 + [hbm] * 4,
+        in_specs=[vmem] * 6 + [hbm] * 9,
         out_specs=(vmem, vmem),
         scratch_shapes=[
+            pltpu.VMEM(expert_rows.shape, bf16),
+            pltpu.VMEM(query_maps.shape, bf16),
+            pltpu.VMEM(key_maps.shape, bf16),
+            pltpu.VMEM(value_rows.shape, bf16),
+            pltpu.VMEM(turns.shape, f32),
             pltpu.VMEM((n_ep, capacity, width), bf16),
             pltpu.VMEM((n_z, row_count, head_width), bf16),
             pltpu.VMEM((n_z, row_count, 2 * head_width), bf16),
@@ -1046,6 +1072,7 @@
             pltpu.VMEM((n_tp, 2, row_count // 2, width), bf16),
             pltpu.VMEM((3, 2, row_count // 2, width), bf16),
             pltpu.VMEM((2, row_count // 2, width), bf16),
+            dma((5,)),
             dma((4,)),
             dma((3 + n_z,)),
             dma((n_ep,)),
@@ -1081,17 +1108,17 @@
         ),
         name="layer",
     )(
-        expert_rows,
         expert_gain.reshape(1, model_width),
         routes.T,
         route_weights.T,
+        offsets,
+        head_lambda.reshape(1, n_z),
+        head_gain.reshape(1, head_width),
+        expert_rows,
         query_maps,
         key_maps,
         value_rows,
         turns,
-        offsets,
-        head_lambda.reshape(1, n_z),
-        head_gain.reshape(1, head_width),
         gate_weight,
         up_weight,
         down_weight,

time: 66.7 us -> 65.1 us (0.976)
  Pallas kernels: 65.2 us -> 64.2 us
    pallas_call x1, Pallas kernels: 63.4 us -> 62.5 us  [fused(): pl.pallas_call(functools.partial(layer_kernel, n_ep, n_tp), out_shape=(ja...]
where the time goes in v4:
time: 65.1 us; the launch traced here: 64.9 us
  Pallas kernels  64.2 us (99%)
    pallas_call x1, Pallas kernels, fused(): pl.pallas_call(functools.partial(layer_kernel, n_ep, n_tp), out_shape=(ja...  62.5 us
    pallas_call x1, Pallas kernels, fused(): pl.pallas_call(hand_over, out_shape=(jax.ShapeDtypeStruct((token_count, w...  1.78 us

profile of v4, /device:TPU:25, one launch (start us, length us, event | category | flops | bytes accessed | tf_op | source)
XLA Modules:
  0.0 64.9 jit_solution(235002459511684307)
XLA Ops:
  0.6 62.5 %layer.1 = (bf16[128,512]{1,0:T(8,128)(2,1)}, bf16[256,512]{1,0:T(8,128)(2,1)}) custom-call(f32[1,2048]{1,0:T(1,128)} %bitcast.5, s32[2,128]{1,0:T(2,128)} %bitcast.6, f32[2,128]{1,0:T(2,128)} %bitcast.7, f32[2,8,128]{2,1,0:T(8,128)} %constant.5.clone.offset_ref, f32[1,4]{1,0:T(1,128)} %bitcast.9, f32[1,256]{1,0:T(1,128)} %bitcast.8, ...), custom_call_target="tpu_custom_call" | custom-call | tf_op jit(solution)/shard_map/layer/pallas_call | solution.py:1030
  63.1 1.8 %hand_over.1 = (bf16[128,512]{1,0:T(8,128)(2,1)}, bf16[256,512]{1,0:T(8,128)(2,1)}) custom-call(bf16[128,512]{1,0:T(8,128)(2,1)} %get-tuple-element.6.expert_ref, bf16[256,512]{1,0:T(8,128)(2,1)} %get-tuple-element.7.mixed_ref), custom_call_target="tpu_custom_call" | custom-call | tf_op jit(solution)/shard_map/hand_over/pallas_call | solution.py:1127

commit v5 on v4

--- a/solution.py
+++ b/solution.py
@@ -855,11 +855,11 @@
 
     sum_part(1)
 
-    def release():
+    def release(steps):
         pl.semaphore_signal(
             hold_sem,
             inc=1,
-            device_id={"ep": lax.rem(ep + n_ep - 2, n_ep)},
+            device_id={"ep": lax.rem(ep + n_ep - 2 * steps, n_ep)},
             device_id_type=MESH,
         )
 
@@ -879,12 +879,12 @@
                 for up in range(middle):
                     for side in range(2):
                         send_cross(up, 0, side, middle + up).wait_send()
+                release(1)
                 pl.semaphore_wait(hold_sem, 1)
-                release()
 
             @pl.when(z != middle - 1)
             def _():
-                pl.semaphore_wait(hold_sem, 1)
+                pl.semaphore_wait(hold_sem, 2)
 
         for target, copy in zip(targets, back):
 
@@ -915,7 +915,8 @@
             with jax.named_scope("held"):
                 for side in range(2):
                     send_cross(0, 1, side, middle + 1).wait_send()
-            release()
+            release(1)
+            release(2)
             for copy in back[part_count:]:
                 copy.start()
 

time: 65.1 us -> 65.1 us (level)
  no operation moved by 1% of the time
where the time goes in v5:
time: 65.1 us; the launch traced here: 64.9 us
  Pallas kernels  64.2 us (99%)
    pallas_call x1, Pallas kernels, fused(): pl.pallas_call(functools.partial(layer_kernel, n_ep, n_tp), out_shape=(ja...  62.5 us
    pallas_call x1, Pallas kernels, fused(): pl.pallas_call(hand_over, out_shape=(jax.ShapeDtypeStruct((token_count, w...  1.78 us

profile of v5, /device:TPU:25, one launch (start us, length us, event | category | flops | bytes accessed | tf_op | source)
XLA Modules:
  0.0 64.9 jit_solution(2934608574575342388)
XLA Ops:
  0.6 62.5 %layer.1 = (bf16[128,512]{1,0:T(8,128)(2,1)}, bf16[256,512]{1,0:T(8,128)(2,1)}) custom-call(f32[1,2048]{1,0:T(1,128)} %bitcast.5, s32[2,128]{1,0:T(2,128)} %bitcast.6, f32[2,128]{1,0:T(2,128)} %bitcast.7, f32[2,8,128]{2,1,0:T(8,128)} %constant.5.clone.offset_ref, f32[1,4]{1,0:T(1,128)} %bitcast.9, f32[1,256]{1,0:T(1,128)} %bitcast.8, ...), custom_call_target="tpu_custom_call" | custom-call | tf_op jit(solution)/shard_map/layer/pallas_call | solution.py:1031
  63.1 1.8 %hand_over.1 = (bf16[128,512]{1,0:T(8,128)(2,1)}, bf16[256,512]{1,0:T(8,128)(2,1)}) custom-call(bf16[128,512]{1,0:T(8,128)(2,1)} %get-tuple-element.6.expert_ref, bf16[256,512]{1,0:T(8,128)(2,1)} %get-tuple-element.7.mixed_ref), custom_call_target="tpu_custom_call" | custom-call | tf_op jit(solution)/shard_map/hand_over/pallas_call | solution.py:1128
